TPU v7x, 256 devices: a whole 4x4x8 slice. The times are simulated.
256 devices in a mesh: ep: 16 (over y, x), tp: 16 (over z, core).
Axes of the slice: x: 4, y: 4, z: 8, core: 2. Of those that a mesh axis runs over, the one named last changes fastest.
Arguments:
- tokens: bfloat16 [1024, 2048], P(('ep', 'tp')), may hold values from -6 to 6
- lengths: int32 [1024], P(('ep', 'tp')), may hold values from 64 to 1024
- cache_latent: bfloat16 [1024, 1024, 512], P(('ep', 'tp')), may hold values from -6 to 6
- cache_rope_key: bfloat16 [1024, 1024, 32], P(('ep', 'tp')), may hold values from -1000 to 1000
- route_ids: int32 [1024, 4], P('ep'), may hold values from 0 to 255, all different within a row; in each aligned block of 64 rows (0 to 63, 64 to 127, ...) at most 2 rows name the same one
- route_weights: float32 [1024, 4], P('ep'), may hold values from 0.2 to 2
- attn_gain: float32 [2048], replicated, may hold values from 0.1 to 1.9
- w_query_nope: bfloat16 [2048, 16, 64], P(None, 'tp'), may hold values from -0.125 to 0.125
- w_query_rope: bfloat16 [2048, 16, 32], P(None, 'tp'), may hold values from -0.125 to 0.125
- w_latent_down: bfloat16 [2048, 512], P(None, 'tp'), may hold values from -0.125 to 0.125
- w_key_rope: bfloat16 [2048, 32], replicated, may hold values from -0.125 to 0.125
- latent_gain: float32 [512], replicated, may hold values from 0.1 to 1.9
- w_key_up: bfloat16 [512, 16, 64], P(None, 'tp'), may hold values from -0.75 to 0.75
- w_value_up: bfloat16 [512, 16, 64], P(None, 'tp'), may hold values from -0.25 to 0.25
- w_attn_out: bfloat16 [16, 64, 2048], P('tp'), may hold values from -0.1875 to 0.1875
- ffn_gain: float32 [2048], replicated, may hold values from 0.1 to 1.9
- expert_gate: bfloat16 [256, 2048, 512], P(('ep', 'tp')), may hold values from -0.125 to 0.125
- expert_up: bfloat16 [256, 2048, 512], P(('ep', 'tp')), may hold values from -0.125 to 0.125
- expert_down: bfloat16 [256, 512, 2048], P(('ep', 'tp')), may hold values from -0.25 to 0.25
- shared_gate: bfloat16 [2048, 512], P(None, 'tp'), may hold values from -0.125 to 0.125
- shared_up: bfloat16 [2048, 512], P(None, 'tp'), may hold values from -0.125 to 0.125
- shared_down: bfloat16 [512, 2048], P('tp'), may hold values from -0.25 to 0.25
- dense_gate: bfloat16 [2048, 1024], P(None, 'tp'), may hold values from -0.125 to 0.125
- dense_up: bfloat16 [2048, 1024], P(None, 'tp'), may hold values from -0.125 to 0.125
- dense_down: bfloat16 [1024, 2048], P('tp'), may hold values from -0.1875 to 0.1875
- branch_gate: bfloat16 [2048], replicated, may hold values from -0.125 to 0.125
Outputs:
- mixed: bfloat16 [1024, 2048], P(('ep', 'tp'))
- new_latent: bfloat16 [1024, 512], P(('ep', 'tp'))
- new_rope_key: bfloat16 [1024, 32], P(('ep', 'tp'))
Inputs may be any that keep to these rules, and one draw needn't show every extreme that they name: `route_ids`: in each aligned block of 64 rows, no expert is named by more than 2 of the block's rows, a bound that some block reaches. Each row names 4 different experts.
All inputs are finite; a program needn't handle non-finite values.
Results may differ from a plain program's by a relative error of at most 0.025.
Values may be sent and summed in bfloat16 or wider, within the bound.
A program may use at most 64 MiB of HBM per device.

v0:
```python
import jax
import jax.numpy as jnp
from jax import lax
from jax.sharding import PartitionSpec as P

epsilon = 1e-06
rope_base = 10000.0


def copy_for_each(shard, axis):
    peers = lax.axis_size(axis)
    return lax.all_to_all(
        jnp.broadcast_to(shard[None], (peers, *shard.shape)), axis, 0, 0, tiled=True
    )


def laid_out(tiles, dim):
    tiles = jnp.moveaxis(tiles, 0, dim)
    lengths = tiles.shape
    return tiles.reshape(*lengths[:dim], lengths[dim] * lengths[dim + 1], *lengths[dim + 2 :])


def collect(shard, axis, dim):
    tiles = copy_for_each(shard, axis)
    return laid_out(tiles, dim)


def sent_together(arrays, axis, split_dim, concat_dim, along):
    ends, at = ([], 0)
    for a in arrays[:-1]:
        at += a.shape[along]
        ends.append(at)
    both = jnp.concatenate(arrays, axis=along)
    return tuple(
        jnp.split(
            lax.all_to_all(both, axis, split_axis=split_dim, concat_axis=concat_dim, tiled=True),
            ends,
            axis=along,
        )
    )


def cut_along(shard, dim, peers):
    before, after = (shard.shape[:dim], shard.shape[dim + 1 :])
    return jnp.moveaxis(shard.reshape(*before, peers, -1, *after), dim, 0)


def sent_and_summed(shard, axis, dim):
    peers = lax.axis_size(axis)
    tiles = lax.all_to_all(cut_along(shard, dim, peers), axis, 0, 0, tiled=True)
    return jnp.sum(tiles.astype(jnp.float32), axis=0)


def norm_rows(values, scales):
    values = values.astype(jnp.float32)
    factor = lax.rsqrt(jnp.mean(values * values, axis=-1, keepdims=True) + epsilon)
    return values * factor * scales


def rotate(values, positions):
    half_dim = values.shape[-1] // 2
    frequencies = rope_base ** (-jnp.arange(half_dim).astype(jnp.float32) / half_dim)
    angles = positions.astype(jnp.float32)[:, None] * frequencies[None, :]
    bcast_shape = (angles.shape[0],) + (1,) * (values.ndim - 2) + (half_dim,)
    cosine = jnp.cos(angles).reshape(bcast_shape)
    sine_val = jnp.sin(angles).reshape(bcast_shape)
    first_half = values[..., :half_dim].astype(jnp.float32)
    second_half = values[..., half_dim:].astype(jnp.float32)
    return jnp.concatenate(
        [
            first_half * cosine - second_half * sine_val,
            first_half * sine_val + second_half * cosine,
        ],
        axis=-1,
    )


def swiglu(inputs, gate_w, up_w):
    gate_val = jnp.dot(inputs, gate_w, preferred_element_type=jnp.float32)
    up_val = jnp.dot(inputs, up_w, preferred_element_type=jnp.float32)
    return (jax.nn.silu(gate_val) * up_val).astype(jnp.bfloat16)


def local(
    tokens,
    lengths,
    cache_latent,
    cache_rope_key,
    route_ids,
    route_weights,
    attn_gain,
    w_query_nope,
    w_query_rope,
    w_latent_down,
    w_key_rope,
    latent_gain,
    w_key_up,
    w_value_up,
    w_attn_out,
    ffn_gain,
    expert_gate,
    expert_up,
    expert_down,
    shared_gate,
    shared_up,
    shared_down,
    dense_gate,
    dense_up,
    dense_down,
    branch_gate,
):
    own_rows, model_width = tokens.shape
    tp_count = lax.axis_size("tp")
    ep_count = lax.axis_size("ep")
    tp_index = lax.axis_index("tp")
    local_heads = w_query_nope.shape[1]
    head_scale = (w_query_nope.shape[2] + w_query_rope.shape[2]) ** (-0.5)
    normed = norm_rows(tokens, attn_gain).astype(jnp.bfloat16)
    group_in = collect(normed, "tp", 0)
    group_rows = group_in.shape[0]
    query_nope = jnp.dot(
        group_in, w_query_nope.reshape(model_width, -1), preferred_element_type=jnp.float32
    )
    query_nope = query_nope.astype(jnp.bfloat16).reshape(group_rows, local_heads, -1)
    query_latent = jnp.einsum(
        "ghn,rhn->ghr", query_nope, w_key_up, preferred_element_type=jnp.float32
    ).astype(jnp.bfloat16)
    query_rope = jnp.dot(
        group_in, w_query_rope.reshape(model_width, -1), preferred_element_type=jnp.float32
    )
    query_rope = query_rope.astype(jnp.bfloat16).reshape(group_rows, local_heads, -1)
    latent_part = jnp.dot(group_in, w_latent_down, preferred_element_type=jnp.float32).astype(
        jnp.bfloat16
    )
    own_latent_q, own_rope_q, latent_raw = (
        *sent_together((query_latent, query_rope), "tp", 0, 1, 2),
        lax.all_to_all(latent_part, "tp", split_axis=0, concat_axis=1, tiled=True),
    )
    new_latent = norm_rows(latent_raw, latent_gain).astype(jnp.bfloat16)
    key_rope = jnp.dot(normed, w_key_rope, preferred_element_type=jnp.float32)
    new_rope = rotate(key_rope, lengths).astype(jnp.bfloat16)
    query_rot = rotate(own_rope_q, lengths).astype(jnp.bfloat16)
    scores = jnp.einsum(
        "bhr,blr->bhl", own_latent_q, cache_latent, preferred_element_type=jnp.float32
    )
    scores = scores + jnp.einsum(
        "bhe,ble->bhl", query_rot, cache_rope_key, preferred_element_type=jnp.float32
    )
    scores = scores * head_scale
    in_range = (
        jnp.arange(cache_latent.shape[1], dtype=jnp.int32)[None, None, :] < lengths[:, None, None]
    )
    scores = jnp.where(in_range, scores, -jnp.inf)
    own_score = jnp.einsum(
        "bhr,br->bh", own_latent_q, new_latent, preferred_element_type=jnp.float32
    )
    own_score = (
        own_score
        + jnp.einsum("bhe,be->bh", query_rot, new_rope, preferred_element_type=jnp.float32)
    ) * head_scale
    peak_score = jnp.maximum(jnp.max(scores, axis=-1), own_score)
    past_exp = jnp.exp(scores - peak_score[..., None])
    own_exp = jnp.exp(own_score - peak_score)
    total_exp = jnp.sum(past_exp, axis=-1) + own_exp
    past_weight = (past_exp / total_exp[..., None]).astype(jnp.bfloat16)
    own_weight = (own_exp / total_exp).astype(jnp.bfloat16)
    out_latent = jnp.einsum(
        "bhl,blr->bhr", past_weight, cache_latent, preferred_element_type=jnp.float32
    )
    out_latent = (
        out_latent
        + own_weight.astype(jnp.float32)[..., None] * new_latent.astype(jnp.float32)[:, None, :]
    )
    out_latent = out_latent.astype(jnp.bfloat16)
    head_latent = lax.all_to_all(out_latent, "tp", split_axis=1, concat_axis=0, tiled=True)
    head_values = jnp.einsum(
        "ghr,rhv->ghv", head_latent, w_value_up, preferred_element_type=jnp.float32
    ).astype(jnp.bfloat16)
    attn_part = jnp.dot(
        head_values.reshape(group_rows, -1),
        w_attn_out.reshape(-1, model_width),
        preferred_element_type=jnp.float32,
    )
    after_attn = tokens.astype(jnp.float32) + sent_and_summed(
        attn_part.astype(jnp.bfloat16), "tp", 0
    )
    own_in = norm_rows(after_attn, ffn_gain).astype(jnp.bfloat16)
    ffn_in = collect(own_in, "tp", 0)
    shared_term = jnp.dot(
        swiglu(ffn_in, shared_gate, shared_up), shared_down, preferred_element_type=jnp.float32
    )
    branch_mix = jax.nn.sigmoid(jnp.dot(ffn_in, branch_gate, preferred_element_type=jnp.float32))
    dense_term = branch_mix[:, None] * jnp.dot(
        swiglu(ffn_in, dense_gate, dense_up), dense_down, preferred_element_type=jnp.float32
    )
    top_count = route_ids.shape[1]
    expert_local = expert_gate.shape[0]
    capacity = max(
        2, (2 * own_rows * top_count + expert_local * ep_count - 1) // (expert_local * ep_count)
    )
    target_count = ep_count * expert_local
    slot_count = target_count * capacity
    column = route_ids // expert_local % tp_count
    target = route_ids // (expert_local * tp_count) * expert_local + route_ids % expert_local
    flat_target = jnp.where(column == tp_index, target, -1).reshape(-1)
    target_hits = (
        flat_target[:, None] == jnp.arange(target_count, dtype=jnp.int32)[None, :]
    ).astype(jnp.int32)
    earlier = jnp.cumsum(target_hits, axis=0) - target_hits
    rank_in = jnp.sum(earlier * target_hits, axis=1)
    slot_index = jnp.where(flat_target >= 0, flat_target * capacity + rank_in, -1).reshape(
        group_rows, top_count
    )
    slot_match = slot_index[:, :, None] == jnp.arange(slot_count, dtype=jnp.int32)[None, None, :]
    dispatch = jnp.any(slot_match, axis=1).astype(jnp.bfloat16)
    combine = jnp.sum(jnp.where(slot_match, route_weights[:, :, None], 0.0), axis=1)
    outgoing = jnp.einsum("gs,gd->sd", dispatch, ffn_in, preferred_element_type=jnp.float32).astype(
        jnp.bfloat16
    )
    outgoing = outgoing.reshape(ep_count, expert_local, capacity, model_width)
    arrived = lax.all_to_all(outgoing, "ep", split_axis=0, concat_axis=0, tiled=True)
    gate_val = jnp.einsum(
        "sxcd,xdf->sxcf", arrived, expert_gate, preferred_element_type=jnp.float32
    )
    up_val = jnp.einsum("sxcd,xdf->sxcf", arrived, expert_up, preferred_element_type=jnp.float32)
    act_val = (jax.nn.silu(gate_val) * up_val).astype(jnp.bfloat16)
    result = jnp.einsum(
        "sxcf,xfd->sxcd", act_val, expert_down, preferred_element_type=jnp.float32
    ).astype(jnp.bfloat16)
    returned = lax.all_to_all(result, "ep", split_axis=0, concat_axis=0, tiled=True)
    routed = jnp.dot(combine, returned.reshape(slot_count, model_width).astype(jnp.float32))
    ffn_total = routed + shared_term + dense_term
    mixed = (after_attn + sent_and_summed(ffn_total.astype(jnp.bfloat16), "tp", 0)).astype(
        jnp.bfloat16
    )
    return (mixed, new_latent, new_rope)


def solution(mesh):
    in_specs = (
        P(("ep", "tp"), None),
        P(("ep", "tp")),
        P(("ep", "tp"), None, None),
        P(("ep", "tp"), None, None),
        P("ep", None),
        P("ep", None),
        P(),
        P(None, "tp", None),
        P(None, "tp", None),
        P(None, "tp"),
        P(),
        P(),
        P(None, "tp", None),
        P(None, "tp", None),
        P("tp", None, None),
        P(),
        P(("ep", "tp"), None, None),
        P(("ep", "tp"), None, None),
        P(("ep", "tp"), None, None),
        P(None, "tp"),
        P(None, "tp"),
        P("tp", None),
        P(None, "tp"),
        P(None, "tp"),
        P("tp", None),
        P(),
    )
    out_specs = (P(("ep", "tp"), None), P(("ep", "tp"), None), P(("ep", "tp"), None))
    return jax.shard_map(local, mesh=mesh, in_specs=in_specs, out_specs=out_specs, check_vma=False)
```

profile of v0, /device:TPU:1, one launch (start us, length us, event | category | flops | bytes accessed | tf_op | source)
XLA Modules:
  0.0 153.4 jit_solution(8097909806356359629)
XLA Ops:
  0.7 1.0 fusion.67
  1.7 0.8 fusion.69
  2.5 0.8 broadcast_in_dim.27
  3.3 10.0 %all-to-all-start = ((bf16[16,4,2048]{2,1,0:T(4,128)(2,1)}), bf16[16,4,2048]{2,1,0:T(4,128)(2,1)S(1)}, u32[]{:S(2)}, u32[]{:S(2)}) async-start(bf16[16,4,2048]{2,1,0:T(4,128)(2,1)} %broadcast_in_dim.27), calls=%async_computation | async-start | bytes 524288 | tf_op jit(solution)/shard_map/all_to_all | solution.py:12
  13.3 0.7 convert_element_type.157
  13.9 1.0 fusion.104
  15.2 0.7 iota_compare_fusion.3
  15.9 8.9 %all-to-all-done = bf16[16,4,2048]{2,1,0:T(4,128)(2,1)S(1)} async-done(((bf16[16,4,2048]{2,1,0:T(4,128)(2,1)}), bf16[16,4,2048]{2,1,0:T(4,128)(2,1)S(1)}, u32[]{:S(2)}, u32[]{:S(2)}) %all-to-all-start) | async-done | bytes 262176 | tf_op jit(solution)/shard_map/all_to_all | solution.py:12
  24.9 1.1 convolution_convert_fusion.7
  26.0 0.7 copy.92
  26.7 3.4 %all-to-all-start.2 = ((bf16[16,4,32]{2,1,0:T(4,128)(2,1)}), bf16[16,4,32]{2,1,0:T(4,128)(2,1)S(1)}, u32[]{:S(2)}, u32[]{:S(2)}) async-start(bf16[16,4,32]{2,1,0:T(4,128)(2,1)} %bitcast.10), calls=%async_computation.2 | async-start | bytes 32768 | tf_op jit(solution)/shard_map/all_to_all | solution.py:137
  30.1 1.1 fusion.28
  31.7 0.5 broadcast.217
  32.2 0.7 reduce.5
  32.8 0.8 reshape.274
  33.6 3.4 %all-to-all-done.2 = bf16[16,4,32]{2,1,0:T(4,128)(2,1)S(1)} async-done(((bf16[16,4,32]{2,1,0:T(4,128)(2,1)}), bf16[16,4,32]{2,1,0:T(4,128)(2,1)S(1)}, u32[]{:S(2)}, u32[]{:S(2)}) %all-to-all-start.2) | async-done | bytes 4128 | tf_op jit(solution)/shard_map/all_to_all | solution.py:137
  37.0 3.7 %all-to-all-start.1 = ((bf16[16,2,1088]{2,1,0:T(2,128)(2,1)}), bf16[16,2,1088]{2,1,0:T(2,128)(2,1)S(1)}, u32[]{:S(2)}, u32[]{:S(2)}) async-start(bf16[16,2,1088]{2,1,0:T(2,128)(2,1)} %reshape.274), calls=%async_computation.1 | async-start | bytes 147456 | tf_op jit(solution)/shard_map/all_to_all | solution.py:36
  41.1 7.7 %all-to-all-done.1 = bf16[16,2,1088]{2,1,0:T(2,128)(2,1)S(1)} async-done(((bf16[16,2,1088]{2,1,0:T(2,128)(2,1)}), bf16[16,2,1088]{2,1,0:T(2,128)(2,1)S(1)}, u32[]{:S(2)}, u32[]{:S(2)}) %all-to-all-start.1) | async-done | bytes 69664 | tf_op jit(solution)/shard_map/all_to_all | solution.py:36
  48.9 0.5 reduce.2
  49.5 3.5 %fusion.60 = f32[4,16,1024]{2,1,0:T(8,128)S(1)} fusion(bf16[4,1024,512]{2,1,0:T(8,128)(2,1)} %param.28, bf16[4,16,544]{2,1,0:T(8,128)(2,1)S(1)} %bitcast.162), kind=kOutput, calls=%fused_computation.67 | convolution fusion | flops 67108864 | bytes 4521984 | tf_op jit(solution)/shard_map/bhr,blr->bhl/dot_general | solution.py:143
  54.0 0.7 fusion.10
  54.7 0.7 copy.94
  55.4 3.4 %all-to-all-start.3 = ((bf16[4,16,512]{2,0,1:T(4,128)(2,1)}), bf16[4,16,512]{2,0,1:T(4,128)(2,1)S(1)}, u32[]{:S(2)}, u32[]{:S(2)}) async-start(bf16[4,16,512]{2,0,1:T(4,128)(2,1)} %copy.94), calls=%async_computation.3 | async-start | bytes 131072 | tf_op jit(solution)/shard_map/all_to_all | solution.py:175
  58.9 7.7 %all-to-all-done.3 = bf16[4,16,512]{2,0,1:T(4,128)(2,1)S(1)} async-done(((bf16[4,16,512]{2,0,1:T(4,128)(2,1)}), bf16[4,16,512]{2,0,1:T(4,128)(2,1)S(1)}, u32[]{:S(2)}, u32[]{:S(2)}) %all-to-all-start.3) | async-done | bytes 65568 | tf_op jit(solution)/shard_map/all_to_all | solution.py:175
  67.0 0.8 reshape.251
  67.8 3.5 %all-to-all-start.4 = ((bf16[16,4,2048]{2,1,0:T(4,128)(2,1)}), bf16[16,4,2048]{2,1,0:T(4,128)(2,1)S(1)}, u32[]{:S(2)}, u32[]{:S(2)}) async-start(bf16[16,4,2048]{2,1,0:T(4,128)(2,1)} %reshape.251), calls=%async_computation.4 | async-start | bytes 524288 | tf_op jit(solution)/shard_map/all_to_all | solution.py:50
  71.6 0.6 reduce-window.6
  72.4 10.7 %all-to-all-done.4 = bf16[16,4,2048]{2,1,0:T(4,128)(2,1)S(1)} async-done(((bf16[16,4,2048]{2,1,0:T(4,128)(2,1)}), bf16[16,4,2048]{2,1,0:T(4,128)(2,1)S(1)}, u32[]{:S(2)}, u32[]{:S(2)}) %all-to-all-start.4) | async-done | bytes 262176 | tf_op jit(solution)/shard_map/all_to_all | solution.py:50
  83.4 0.8 broadcast_in_dim.31
  84.2 3.4 %all-to-all-start.5 = ((bf16[16,4,2048]{2,1,0:T(4,128)(2,1)}), bf16[16,4,2048]{2,1,0:T(4,128)(2,1)S(1)}, u32[]{:S(2)}, u32[]{:S(2)}) async-start(bf16[16,4,2048]{2,1,0:T(4,128)(2,1)} %broadcast_in_dim.31), calls=%async_computation.5 | async-start | bytes 524288 | tf_op jit(solution)/shard_map/all_to_all | solution.py:12
  88.0 10.5 %all-to-all-done.5 = bf16[16,4,2048]{2,1,0:T(4,128)(2,1)S(1)} async-done(((bf16[16,4,2048]{2,1,0:T(4,128)(2,1)}), bf16[16,4,2048]{2,1,0:T(4,128)(2,1)S(1)}, u32[]{:S(2)}, u32[]{:S(2)}) %all-to-all-start.5) | async-done | bytes 262176 | tf_op jit(solution)/shard_map/all_to_all | solution.py:12
  99.2 0.7 reshape.254
  100.0 6.8 %all-to-all-start.6 = ((bf16[16,1,2,2048]{3,2,1,0:T(2,128)(2,1)}), bf16[16,1,2,2048]{3,2,1,0:T(2,128)(2,1)S(1)}, u32[]{:S(2)}, u32[]{:S(2)}) async-start(bf16[16,1,2,2048]{3,2,1,0:T(2,128)(2,1)} %bitcast.23), calls=%async_computation.6 | async-start | bytes 262144 | tf_op jit(solution)/shard_map/all_to_all | solution.py:221
  106.7 1.5 convolution_multiply_fusion
  108.2 5.7 %all-to-all-done.6 = bf16[16,1,2,2048]{3,2,1,0:T(2,128)(2,1)S(1)} async-done(((bf16[16,1,2,2048]{3,2,1,0:T(2,128)(2,1)}), bf16[16,1,2,2048]{3,2,1,0:T(2,128)(2,1)S(1)}, u32[]{:S(2)}, u32[]{:S(2)}) %all-to-all-start.6) | async-done | bytes 131104 | tf_op jit(solution)/shard_map/all_to_all | solution.py:221
  113.9 2.0 %fusion.12 = f32[16,1,2,512]{3,0,2,1:T(8,128)S(1)} fusion(bf16[1,2048,512]{2,1,0:T(8,128)(2,1)} %param.42, bf16[16,1,2,2048]{3,2,1,0:T(2,128)(2,1)S(1)} %all-to-all-done.6), kind=kOutput, calls=%fused_computation.20 | convolution fusion | flops 67108864 | bytes 2293760 | tf_op jit(solution)/shard_map/sxcd,xdf->sxcf/dot_general | solution.py:222
  115.9 2.5 %fusion.2 = bf16[16,1,2,2048]{3,0,2,1:T(8,128)(2,1)S(1)} fusion(bf16[1,512,2048]{2,1,0:T(8,128)(2,1)S(1)} %copy-done, bf16[1,2048,512]{2,1,0:T(8,128)(2,1)} %param.43, bf16[16,1,2,2048]{3,2,1,0:T(2,128)(2,1)S(1)} %all-to-all-done.6, f32[16,1,2,512]{3,0,2,1:T(8,128)S(1)} %fusion.12), kind=kOutput, calls=%fused_computation.7 | convolution fusion | flops 134381568 | bytes 4521984 | tf_op jit(solution)/shard_map/sxcf,xfd->sxcd/dot_general | solution.py:227
  118.5 0.8 copy.103
  119.3 3.5 %all-to-all-start.7 = ((bf16[16,1,2,2048]{3,2,1,0:T(2,128)(2,1)}), bf16[16,1,2,2048]{3,2,1,0:T(2,128)(2,1)S(1)}, u32[]{:S(2)}, u32[]{:S(2)}) async-start(bf16[16,1,2,2048]{3,2,1,0:T(2,128)(2,1)} %copy.103), calls=%async_computation.7 | async-start | bytes 262144 | tf_op jit(solution)/shard_map/all_to_all | solution.py:230
  123.0 6.7 %all-to-all-done.7 = bf16[16,1,2,2048]{3,2,1,0:T(2,128)(2,1)S(1)} async-done(((bf16[16,1,2,2048]{3,2,1,0:T(2,128)(2,1)}), bf16[16,1,2,2048]{3,2,1,0:T(2,128)(2,1)S(1)}, u32[]{:S(2)}, u32[]{:S(2)}) %all-to-all-start.7) | async-done | bytes 131104 | tf_op jit(solution)/shard_map/all_to_all | solution.py:230
  129.6 0.7 reshape.260
  130.3 1.1 fusion.105
  131.5 2.2 %fusion.1 = bf16[64,2048]{1,0:T(8,128)(2,1)} fusion(f32[64,2048]{1,0:T(8,128)S(1)} %convolution_multiply_fusion, f32[64,2048]{1,0:T(8,128)S(1)} %fusion.105, bf16[32,2048]{1,0:T(8,128)(2,1)} %param.47, bf16[64,2048]{1,0:T(8,128)(2,1)S(1)} %reshape.253, bf16[2048,32]{0,1:T(8,128)(2,1)} %param.46, f32[64,32]{0,1:T(8,128)S(1)} %fusion.106), kind=kOutput, calls=%fused_computation.3 | convolution fusion | flops 17182720 | bytes 1843200 | tf_op jit(solution)/shard_map/dot_general | solution.py:189
  133.7 1.8 %reshape.261 = bf16[16,4,2048]{2,1,0:T(4,128)(2,1)} reshape(bf16[64,2048]{1,0:T(8,128)(2,1)} %fusion.1) | data formatting | bytes 524288 | tf_op jit(solution)/shard_map/reshape | solution.py:45
  135.5 5.5 %all-to-all-start.8 = ((bf16[16,4,2048]{2,1,0:T(4,128)(2,1)}), bf16[16,4,2048]{2,1,0:T(4,128)(2,1)S(1)}, u32[]{:S(2)}, u32[]{:S(2)}) async-start(bf16[16,4,2048]{2,1,0:T(4,128)(2,1)} %reshape.261), calls=%async_computation.8 | async-start | bytes 524288 | tf_op jit(solution)/shard_map/all_to_all | solution.py:50
  140.9 0.6 pad_maximum_fusion.4
  141.6 11.1 %all-to-all-done.8 = bf16[16,4,2048]{2,1,0:T(4,128)(2,1)S(1)} async-done(((bf16[16,4,2048]{2,1,0:T(4,128)(2,1)}), bf16[16,4,2048]{2,1,0:T(4,128)(2,1)S(1)}, u32[]{:S(2)}, u32[]{:S(2)}) %all-to-all-start.8) | async-done | bytes 262176 | tf_op jit(solution)/shard_map/all_to_all | solution.py:50
  152.8 0.6 add_convert_fusion
  (84 shorter events, 4.8 us)
Async XLA Ops:
  0.6 115.3 %copy-start = (bf16[1,512,2048]{2,1,0:T(8,128)(2,1)S(1)}, bf16[1,512,2048]{2,1,0:T(8,128)(2,1)}, u32[]{:S(2)}) copy-start(bf16[1,512,2048]{2,1,0:T(8,128)(2,1)} %param.44) | copy-start | bytes 6291460
  0.6 30.6 %copy-start.9 = (bf16[512,1,64]{0,2,1:T(8,128)(2,1)S(1)}, bf16[512,1,64]{0,2,1:T(8,128)(2,1)}, u32[]{:S(2)}) copy-start(bf16[512,1,64]{0,2,1:T(8,128)(2,1)} %param.38) | copy-start | bytes 196612
  0.7 30.6 %copy-start.5 = (bf16[2048,1,64]{0,2,1:T(8,128)(2,1)S(1)}, bf16[2048,1,64]{0,2,1:T(8,128)(2,1)}, u32[]{:S(2)}) copy-start(bf16[2048,1,64]{0,2,1:T(8,128)(2,1)} %param.33) | copy-start | bytes 786436
  0.7 40.3 %copy-start.14 = (f32[512]{0:T(512)S(1)}, f32[512]{0:T(512)}, u32[]{:S(2)}) copy-start(f32[512]{0:T(512)} %param.37) | copy-start | bytes 6148
  3.3 21.6 %all-to-all-start = ((bf16[16,4,2048]{2,1,0:T(4,128)(2,1)}), bf16[16,4,2048]{2,1,0:T(4,128)(2,1)S(1)}, u32[]{:S(2)}, u32[]{:S(2)}) async-start(bf16[16,4,2048]{2,1,0:T(4,128)(2,1)} %broadcast_in_dim.27), calls=%async_computation | async-start | bytes 524288 | tf_op jit(solution)/shard_map/all_to_all | solution.py:12
  26.7 10.3 %all-to-all-start.2 = ((bf16[16,4,32]{2,1,0:T(4,128)(2,1)}), bf16[16,4,32]{2,1,0:T(4,128)(2,1)S(1)}, u32[]{:S(2)}, u32[]{:S(2)}) async-start(bf16[16,4,32]{2,1,0:T(4,128)(2,1)} %bitcast.10), calls=%async_computation.2 | async-start | bytes 32768 | tf_op jit(solution)/shard_map/all_to_all | solution.py:137
  37.0 11.7 %all-to-all-start.1 = ((bf16[16,2,1088]{2,1,0:T(2,128)(2,1)}), bf16[16,2,1088]{2,1,0:T(2,128)(2,1)S(1)}, u32[]{:S(2)}, u32[]{:S(2)}) async-start(bf16[16,2,1088]{2,1,0:T(2,128)(2,1)} %reshape.274), calls=%async_computation.1 | async-start | bytes 147456 | tf_op jit(solution)/shard_map/all_to_all | solution.py:36
  41.1 12.0 %copy-start.13 = (bf16[4,512]{1,0:T(4,128)(2,1)}, bf16[4,512]{1,0:T(4,128)(2,1)S(1)}, u32[]{:S(2)}) copy-start(bf16[4,512]{1,0:T(4,128)(2,1)S(1)} %get-tuple-element.4) | copy-start | bytes 12292
  49.5 3.8 %copy-start.3 = (bf16[4,1024,32]{1,2,0:T(8,128)(2,1)S(1)}, bf16[4,1024,32]{1,2,0:T(8,128)(2,1)}, u32[]{:S(2)}) copy-start(bf16[4,1024,32]{1,2,0:T(8,128)(2,1)} %param.29) | copy-start | bytes 786436
  49.5 4.4 %copy-start.1 = (bf16[4,1024,512]{2,1,0:T(8,128)(2,1)S(1)}, bf16[4,1024,512]{2,1,0:T(8,128)(2,1)}, u32[]{:S(2)}) copy-start(bf16[4,1024,512]{2,1,0:T(8,128)(2,1)} %param.28) | copy-start | bytes 12582916
  53.9 4.9 %copy-start.15 = (s32[64,4]{0,1:T(4,128)S(1)}, s32[64,4]{0,1:T(4,128)}, u32[]{:S(2)}) copy-start(s32[64,4]{0,1:T(4,128)} %param.30) | copy-start | bytes 3076
  53.9 12.7 %copy-start.6 = (bf16[1,64,2048]{2,1,0:T(8,128)(2,1)S(1)}, bf16[1,64,2048]{2,1,0:T(8,128)(2,1)}, u32[]{:S(2)}) copy-start(bf16[1,64,2048]{2,1,0:T(8,128)(2,1)} %param.40) | copy-start | bytes 786436
  54.0 12.7 %copy-start.10 = (bf16[512,1,64]{0,2,1:T(8,128)(2,1)S(1)}, bf16[512,1,64]{0,2,1:T(8,128)(2,1)}, u32[]{:S(2)}) copy-start(bf16[512,1,64]{0,2,1:T(8,128)(2,1)} %param.39) | copy-start | bytes 196612
  54.7 28.5 %copy-start.2 = (bf16[4,2048]{1,0:T(4,128)(2,1)S(1)}, bf16[4,2048]{1,0:T(4,128)(2,1)}, u32[]{:S(2)}) copy-start(bf16[4,2048]{1,0:T(4,128)(2,1)} %param.26) | copy-start | bytes 49156
  54.7 28.6 %copy-start.11 = (f32[2048]{0:T(1024)S(1)}, f32[2048]{0:T(1024)}, u32[]{:S(2)}) copy-start(f32[2048]{0:T(1024)} %param.41) | copy-start | bytes 24580
  54.7 33.0 %copy-start.12 = (bf16[2048]{0:T(1024)(128)(2,1)S(1)}, bf16[2048]{0:T(1024)(128)(2,1)}, u32[]{:S(2)}) copy-start(bf16[2048]{0:T(1024)(128)(2,1)} %param.51) | copy-start | bytes 12292
  54.7 33.3 %copy-start.16 = (f32[64,4]{0,1:T(4,128)S(1)}, f32[64,4]{0,1:T(4,128)}, u32[]{:S(2)}) copy-start(f32[64,4]{0,1:T(4,128)} %param.31) | copy-start | bytes 3076
  55.4 11.2 %all-to-all-start.3 = ((bf16[4,16,512]{2,0,1:T(4,128)(2,1)}), bf16[4,16,512]{2,0,1:T(4,128)(2,1)S(1)}, u32[]{:S(2)}, u32[]{:S(2)}) async-start(bf16[4,16,512]{2,0,1:T(4,128)(2,1)} %copy.94), calls=%async_computation.3 | async-start | bytes 131072 | tf_op jit(solution)/shard_map/all_to_all | solution.py:175
  67.0 31.8 %copy-start.7 = (bf16[2048,64]{0,1:T(8,128)(2,1)S(1)}, bf16[2048,64]{0,1:T(8,128)(2,1)}, u32[]{:S(2)}) copy-start(bf16[2048,64]{0,1:T(8,128)(2,1)} %param.48) | copy-start | bytes 786436
  67.8 15.2 %all-to-all-start.4 = ((bf16[16,4,2048]{2,1,0:T(4,128)(2,1)}), bf16[16,4,2048]{2,1,0:T(4,128)(2,1)S(1)}, u32[]{:S(2)}, u32[]{:S(2)}) async-start(bf16[16,4,2048]{2,1,0:T(4,128)(2,1)} %reshape.251), calls=%async_computation.4 | async-start | bytes 524288 | tf_op jit(solution)/shard_map/all_to_all | solution.py:50
  71.3 35.4 %copy-start.4 = (bf16[64,2048]{1,0:T(8,128)(2,1)S(1)}, bf16[64,2048]{1,0:T(8,128)(2,1)}, u32[]{:S(2)}) copy-start(bf16[64,2048]{1,0:T(8,128)(2,1)} %param.50) | copy-start | bytes 786436
  84.2 14.4 %all-to-all-start.5 = ((bf16[16,4,2048]{2,1,0:T(4,128)(2,1)}), bf16[16,4,2048]{2,1,0:T(4,128)(2,1)S(1)}, u32[]{:S(2)}, u32[]{:S(2)}) async-start(bf16[16,4,2048]{2,1,0:T(4,128)(2,1)} %broadcast_in_dim.31), calls=%async_computation.5 | async-start | bytes 524288 | tf_op jit(solution)/shard_map/all_to_all | solution.py:12
  100.0 13.9 %all-to-all-start.6 = ((bf16[16,1,2,2048]{3,2,1,0:T(2,128)(2,1)}), bf16[16,1,2,2048]{3,2,1,0:T(2,128)(2,1)S(1)}, u32[]{:S(2)}, u32[]{:S(2)}) async-start(bf16[16,1,2,2048]{3,2,1,0:T(2,128)(2,1)} %bitcast.23), calls=%async_computation.6 | async-start | bytes 262144 | tf_op jit(solution)/shard_map/all_to_all | solution.py:221
  115.9 6.8 %copy-start.8 = (bf16[2048,32]{0,1:T(8,128)(2,1)S(1)}, bf16[2048,32]{0,1:T(8,128)(2,1)}, u32[]{:S(2)}) copy-start(bf16[2048,32]{0,1:T(8,128)(2,1)} %param.45) | copy-start | bytes 393220
  119.3 10.4 %all-to-all-start.7 = ((bf16[16,1,2,2048]{3,2,1,0:T(2,128)(2,1)}), bf16[16,1,2,2048]{3,2,1,0:T(2,128)(2,1)S(1)}, u32[]{:S(2)}, u32[]{:S(2)}) async-start(bf16[16,1,2,2048]{3,2,1,0:T(2,128)(2,1)} %copy.103), calls=%async_computation.7 | async-start | bytes 262144 | tf_op jit(solution)/shard_map/all_to_all | solution.py:230
  135.5 17.2 %all-to-all-start.8 = ((bf16[16,4,2048]{2,1,0:T(4,128)(2,1)}), bf16[16,4,2048]{2,1,0:T(4,128)(2,1)S(1)}, u32[]{:S(2)}, u32[]{:S(2)}) async-start(bf16[16,4,2048]{2,1,0:T(4,128)(2,1)} %reshape.261), calls=%async_computation.8 | async-start | bytes 524288 | tf_op jit(solution)/shard_map/all_to_all | solution.py:50
where the time goes:
time: 155 us; the launch traced here: 153 us
  waiting for transfers between devices  72.4 us (47%)
  starting transfers between devices  43.1 us (28%)
  matrix products  19 us (12%)
  local copies, waits for them, and re-layouts  10.2 us (7%)
  other arithmetic  7.66 us (5%)
    all_to_all x2, waiting for transfers between devices, sent_and_summed(): tiles = lax.all_to_all(cut_along(shard, dim, peers), axis, 0, 0, tiled=True)  21.8 us
    all_to_all x2, waiting for transfers between devices, copy_for_each(): lax.all_to_all(jnp.broadcast_to(shard[None], (peers, *shard.shape)), axis...  19.5 us
    all_to_all x2, starting transfers between devices, copy_for_each(): lax.all_to_all(jnp.broadcast_to(shard[None], (peers, *shard.shape)), axis...  13.4 us
    all_to_all x2, starting transfers between devices, sent_and_summed(): tiles = lax.all_to_all(cut_along(shard, dim, peers), axis, 0, 0, tiled=True)  8.98 us
    all_to_all x1, waiting for transfers between devices, local(): lax.all_to_all(out_latent, 'tp', split_axis=1, concat_axis=0, tiled=True)  7.69 us
    all_to_all x1, waiting for transfers between devices, sent_together(): lax.all_to_all(both, axis, split_axis=split_dim, concat_axis=concat_dim,...  7.66 us
    all_to_all x1, starting transfers between devices, local(): lax.all_to_all(outgoing, 'ep', split_axis=0, concat_axis=0, tiled=True)  6.75 us
    all_to_all x1, waiting for transfers between devices, local(): lax.all_to_all(result, 'ep', split_axis=0, concat_axis=0, tiled=True)  6.66 us
  transfers between devices with their start and end apart: 9, of which 9 were waited for; matrix products, arithmetic and copies ran while one was open for 7% of the time, Pallas kernels for 0%

commit v1 on v0

v1 whole, which is shorter than its diff:
```python
import functools

import jax
import jax.numpy as jnp
from jax import lax
from jax.experimental import pallas as pl
from jax.experimental.pallas import tpu as pltpu
from jax.sharding import PartitionSpec as P

EPS = 1e-06
ROPE_BASE = 10000.0
MESH = pl.DeviceIdType.MESH
F32 = jnp.float32
BF16 = jnp.bfloat16


def nn(a, b):
    return lax.dot_general(a, b, (((1,), (0,)), ((), ())), preferred_element_type=F32)


def nt(a, b):
    return lax.dot_general(a, b, (((1,), (1,)), ((), ())), preferred_element_type=F32)


def tn(a, b):
    return lax.dot_general(a, b, (((0,), (0,)), ((), ())), preferred_element_type=F32)


def normed_rows(x, gain):
    return x * lax.rsqrt(jnp.mean(x * x, axis=-1, keepdims=True) + EPS) * gain


def silu(v):
    return v / (1.0 + jnp.exp(-v))


def layer_kernel(
    n_tp,
    n_ep,
    lengths,
    tokens,
    cache_h,
    rope_h,
    ids_h,
    rw_h,
    again_h,
    wqn_h,
    wqr_h,
    wld_h,
    wkr_h,
    lgain_h,
    wku_h,
    wvu_h,
    wao_h,
    fgain_h,
    eg_h,
    eu_h,
    ed_h,
    sg_h,
    su_h,
    sd_h,
    dg_h,
    du_h,
    dd_h,
    bg_h,
    mixed_o,
    nlat_o,
    nrope_o,
    cache,
    rope,
    ids,
    rw,
    again,
    w1,
    wkr,
    lgain,
    wku,
    wvu,
    wao,
    fgain,
    eg,
    eu,
    ed,
    w2,
    sd,
    dd,
    bg,
    xa,
    bs,
    br,
    cs,
    cr,
    ds_,
    dr,
    ee,
    fs,
    fr,
    gs,
    gr,
    hs,
    hr,
    big,
    small,
    rf,
    krs,
    lsem,
    send,
    recv,
):
    me = lax.axis_index("tp")
    grp = lax.axis_index("ep")
    rows, width = tokens.shape
    group = rows * n_tp
    nope = wqn_h.shape[0]
    ropew = wqr_h.shape[0]
    latw = wld_h.shape[0]
    latent = wku_h.shape[1]
    length = cache.shape[1]
    scale = (nope + ropew) ** (-0.5)

    wide = latent + 128

    def put(where, value):
        for k in range(value.shape[1] // 128):
            rf[k, where, :] = value[:, 128 * k : 128 * k + 128]

    def get(where, columns):
        return jnp.concatenate([rf[k, where, :] for k in range(columns // 128)], axis=1)

    jobs = [
        (tokens, xa.at[me]),
        (again_h, again),
        (wqn_h, w1.at[pl.ds(0, nope)]),
        (wqr_h, w1.at[pl.ds(nope, ropew)]),
        (wld_h, w1.at[pl.ds(nope + ropew, latw)]),
        (wkr_h, wkr),
        (wku_h, wku),
        (lgain_h, lgain),
        (cache_h, cache),
        (rope_h, rope),
        (wvu_h, wvu),
        (wao_h, wao),
        (fgain_h, fgain),
        (ids_h, ids),
        (rw_h, rw),
        (bg_h, bg),
        (sg_h, w2.at[pl.ds(0, sg_h.shape[0])]),
        (su_h, w2.at[pl.ds(sg_h.shape[0], sg_h.shape[0])]),
        (dg_h, w2.at[pl.ds(2 * sg_h.shape[0], dg_h.shape[0])]),
        (du_h, w2.at[pl.ds(2 * sg_h.shape[0] + dg_h.shape[0], dg_h.shape[0])]),
        (eg_h, eg),
        (eu_h, eu),
        (ed_h, ed),
        (sd_h, sd),
        (dd_h, dd),
    ]
    local = [pltpu.make_async_copy(s, d, lsem.at[i]) for i, (s, d) in enumerate(jobs)]
    for c in local:
        c.start()

    barrier = pltpu.get_barrier_semaphore()

    def greet(i, _):
        pl.semaphore_signal(
            barrier, inc=1, device_id={"tp": lax.rem(me + i, n_tp)}, device_id_type=MESH
        )
        return 0

    def greet_ep(i, _):
        pl.semaphore_signal(
            barrier, inc=1, device_id={"ep": lax.rem(grp + i, n_ep)}, device_id_type=MESH
        )
        return 0

    lax.fori_loop(1, n_tp, greet, 0)
    lax.fori_loop(1, n_ep, greet_ep, 0)

    def hop(phase, i, axis, n, mine, src, dst):
        to = lax.rem(mine + i, n)
        return pltpu.make_async_remote_copy(
            src_ref=src(to),
            dst_ref=dst.at[mine],
            send_sem=send.at[phase, i],
            recv_sem=recv.at[phase, i],
            device_id={axis: to},
            device_id_type=MESH,
        )

    def start_all(phase, axis, n, mine, src, dst):
        def body(i, _):
            hop(phase, i, axis, n, mine, src, dst).start()
            return 0

        lax.fori_loop(1, n, body, 0)

    def wait_all(phase, axis, n, mine, src, dst):
        def body(i, _):
            hop(phase, i, axis, n, mine, src, dst).wait_recv()
            return 0

        lax.fori_loop(1, n, body, 0)

    def wait_sent(phase, axis, n, mine, src, dst):
        def body(i, _):
            hop(phase, i, axis, n, mine, src, dst).wait_send()
            return 0

        lax.fori_loop(1, n, body, 0)

    ex = [
        (0, "tp", n_tp, me, lambda to: xa.at[me], xa),
        (1, "tp", n_tp, me, lambda to: bs.at[to], br),
        (2, "tp", n_tp, me, lambda to: cs.at[to], cr),
        (3, "tp", n_tp, me, lambda to: ds_.at[to], dr),
        (4, "tp", n_tp, me, lambda to: ee.at[me], ee),
        (5, "ep", n_ep, grp, lambda to: fs.at[to], fr),
        (6, "ep", n_ep, grp, lambda to: gs.at[to], gr),
        (7, "tp", n_tp, me, lambda to: hs.at[to], hr),
    ]

    lane = lax.broadcasted_iota(jnp.int32, (rows, 128), 1)
    rowi = lax.broadcasted_iota(jnp.int32, (rows, 128), 0)
    half = ropew // 2
    freq = jnp.zeros((rows, 128), F32)
    for i in range(half):
        freq = jnp.where(lane % half == i, F32(ROPE_BASE ** (-i / half)), freq)
    pos = jnp.zeros((rows, 128), jnp.int32)
    for s in range(rows):
        pos = jnp.where(rowi == s, lengths[s], pos)
    angle = pos.astype(F32) * freq
    cosv = jnp.cos(angle)
    sinv = jnp.sin(angle)

    def rotated(v, c, s):
        ln = lax.broadcasted_iota(jnp.int32, v.shape, 1)
        other = jnp.where(
            ln % ropew < half, -pltpu.roll(v, 128 - half, 1), pltpu.roll(v, half, 1)
        )
        return v * c + other * s

    pl.semaphore_wait(barrier, (n_tp - 1) + (n_ep - 1))
    local[0].wait()
    start_all(*ex[0])

    local[1].wait()
    local[5].wait()
    tok = xa[me].astype(F32)
    own_normed = normed_rows(tok, again[...]).astype(BF16)
    krs[...] = jnp.zeros_like(krs)
    krs[:, 0:ropew] = nt(own_normed, wkr[...])
    new_rope = rotated(krs[...], cosv, sinv).astype(BF16).astype(F32)
    nrope_o[...] = new_rope[:, 0:ropew].astype(BF16)
    for i in (2, 3, 4, 6, 7):
        local[i].wait()

    wait_all(*ex[0])
    for t in range(n_tp):
        big[pl.ds(rows * t, rows), :] = xa[t].astype(F32)
    normed = normed_rows(big[...], again[...]).astype(BF16)
    y = nt(normed, w1[...])
    ql = nn(y[:, 0:nope].astype(BF16), wku[...])
    put(pl.ds(0, group), jnp.concatenate([ql, y], axis=1))
    for t in range(n_tp):
        bs[t] = get(pl.ds(rows * t, rows), wide).astype(BF16)
    start_all(*ex[1])
    br[me] = bs[me]
    wait_all(*ex[1])
    for t in range(n_tp):
        put(pl.ds(rows * t, rows), br[t].astype(F32))

    parts = []
    ln4 = lax.broadcasted_iota(jnp.int32, (rows, 128), 1)
    per = 128 // latw
    for k in range(latent // 128):
        acc = jnp.zeros((rows, 128), F32)
        for j in range(per):
            piece = br[k * per + j][:, latent : latent + 128].astype(F32)
            shift = (j * latw - (nope + ropew)) % 128
            if shift:
                piece = pltpu.roll(piece, shift, 1)
            acc = jnp.where(ln4 // latw == j, piece, acc)
        parts.append(acc)
    latent_raw = jnp.concatenate(parts, axis=1)
    nl16 = normed_rows(latent_raw, lgain[...]).astype(BF16)
    nlat_o[...] = nl16
    new_latent = nl16.astype(F32)
    lane_r = lax.broadcasted_iota(jnp.int32, (rows, 128), 1)
    nr_al = jnp.where(
        (lane_r >= nope) & (lane_r < nope + ropew), pltpu.roll(new_rope, nope, 1), 0.0
    )

    local[8].wait()
    local[9].wait()
    n_heads = n_tp
    outs = []
    for s in range(rows):
        q = get(pl.ds(s, n_heads, stride=rows), latent)
        qr = rf[latent // 128, pl.ds(s, n_heads, stride=rows), :]
        qrot = rotated(qr, cosv[s : s + 1], sinv[s : s + 1]).astype(BF16)
        sc = nt(q.astype(BF16), cache[s])
        sc = (sc + nn(qrot[:, nope : nope + ropew], rope[s])) * scale
        col = lax.broadcasted_iota(jnp.int32, (n_heads, length), 1)
        sc = jnp.where(col < lengths[s], sc, -jnp.inf)
        nls = new_latent[s : s + 1]
        own = (
            jnp.sum(q * nls, axis=-1, keepdims=True)
            + jnp.sum(qrot.astype(F32) * nr_al[s : s + 1], axis=-1, keepdims=True)
        ) * scale
        peak = jnp.maximum(jnp.max(sc, axis=-1, keepdims=True), own)
        pe = jnp.exp(sc - peak)
        oe = jnp.exp(own - peak)
        inv = 1.0 / (jnp.sum(pe, axis=-1, keepdims=True) + oe)
        pw = (pe * inv).astype(BF16)
        ow = (oe * inv).astype(BF16).astype(F32)
        outs.append(nn(pw, cache[s]) + ow * nls)
    for s in range(rows):
        put(pl.ds(s, n_heads, stride=rows), outs[s])
    for t in range(n_tp):
        cs[t] = get(pl.ds(rows * t, rows), latent).astype(BF16)
    start_all(*ex[2])
    cr[me] = cs[me]
    for i in range(10, 16):
        local[i].wait()

    cap = fs.shape[1]
    slots = n_ep * cap
    sl = lax.broadcasted_iota(jnp.int32, (slots, group), 0)
    want = (sl // cap) * n_tp + me
    hit = jnp.zeros((slots, group), F32)
    wgt = jnp.zeros((slots, group), F32)
    for k in range(ids_h.shape[0]):
        m = ids[k : k + 1, :] == want
        hit = jnp.where(m, 1.0, hit)
        wgt = jnp.where(m, rw[k : k + 1, :], wgt)
    before = (
        lax.broadcasted_iota(jnp.int32, (group, group), 0)
        < lax.broadcasted_iota(jnp.int32, (group, group), 1)
    )
    rank = nn(hit.astype(BF16), jnp.where(before, 1.0, 0.0).astype(BF16))
    taken = (hit > 0.5) & (jnp.abs(rank - (sl % cap).astype(F32)) < 0.5)
    disp = jnp.where(taken, 1.0, 0.0).astype(BF16)
    comb = jnp.where(taken, wgt, 0.0)
    comb_hi = comb.astype(BF16)
    comb_lo = (comb - comb_hi.astype(F32)).astype(BF16)

    wait_all(*ex[2])
    for t in range(n_tp):
        put(pl.ds(rows * t, rows), cr[t].astype(F32))
    hv = nt(get(pl.ds(0, group), latent).astype(BF16), wvu[...]).astype(BF16)
    big[...] = nn(hv, wao[...])
    for t in range(n_tp):
        ds_[t] = big[pl.ds(rows * t, rows), :].astype(BF16)
    start_all(*ex[3])
    dr[me] = ds_[me]
    for i in range(16, len(jobs)):
        local[i].wait()
    wait_all(*ex[3])
    after = tok
    total = jnp.zeros_like(tok)
    for t in range(n_tp):
        total = total + dr[t].astype(F32)
    after = tok + total
    ee[me] = normed_rows(after, fgain[...]).astype(BF16)
    start_all(*ex[4])
    wait_all(*ex[4])
    for t in range(n_tp):
        big[pl.ds(rows * t, rows), :] = ee[t].astype(F32)
    ffn = big[...].astype(BF16)
    out = nn(disp, ffn)
    mix = jax.nn.sigmoid(jnp.sum(big[...] * bg[...], axis=-1, keepdims=True))
    small[...] = out
    for g in range(n_ep):
        fs[g] = small[pl.ds(cap * g, cap), :].astype(BF16)
    start_all(*ex[5])
    fr[grp] = fs[grp]
    h = nt(ffn, w2[...])
    a, b = sg_h.shape[0], dg_h.shape[0]
    sact = (silu(h[:, 0:a]) * h[:, a : 2 * a]).astype(BF16)
    dact = (silu(h[:, 2 * a : 2 * a + b]) * h[:, 2 * a + b : 2 * a + 2 * b]).astype(BF16)
    wait_all(*ex[5])
    for g in range(n_ep):
        small[pl.ds(cap * g, cap), :] = fr[g].astype(F32)
    arrived = small[...].astype(BF16)
    act = (silu(nn(arrived, eg[...])) * nn(arrived, eu[...])).astype(BF16)
    small[...] = nn(act, ed[...])
    for g in range(n_ep):
        gs[g] = small[pl.ds(cap * g, cap), :].astype(BF16)
    start_all(*ex[6])
    gr[grp] = gs[grp]
    big[...] = nn(sact, sd[...]) + mix * nn(dact, dd[...])
    wait_all(*ex[6])
    for g in range(n_ep):
        small[pl.ds(cap * g, cap), :] = gr[g].astype(F32)
    back = small[...].astype(BF16)
    big[...] += tn(comb_hi, back) + tn(comb_lo, back)
    for t in range(n_tp):
        hs[t] = big[pl.ds(rows * t, rows), :].astype(BF16)
    start_all(*ex[7])
    hr[me] = hs[me]
    for e in ex[:7]:
        wait_sent(*e)
    wait_all(*ex[7])
    total = jnp.zeros_like(tok)
    for t in range(n_tp):
        total = total + hr[t].astype(F32)
    mixed_o[...] = (after + total).astype(BF16)
    wait_sent(*ex[7])


def local(
    tokens,
    lengths,
    cache_latent,
    cache_rope_key,
    route_ids,
    route_weights,
    attn_gain,
    w_query_nope,
    w_query_rope,
    w_latent_down,
    w_key_rope,
    latent_gain,
    w_key_up,
    w_value_up,
    w_attn_out,
    ffn_gain,
    expert_gate,
    expert_up,
    expert_down,
    shared_gate,
    shared_up,
    shared_down,
    dense_gate,
    dense_up,
    dense_down,
    branch_gate,
):
    n_tp = lax.axis_size("tp")
    n_ep = lax.axis_size("ep")
    rows, width = tokens.shape
    group = rows * n_tp
    wqn = w_query_nope.reshape(width, -1).T
    wqr = w_query_rope.reshape(width, -1).T
    wld = w_latent_down.T
    wkr = w_key_rope.T
    wku = w_key_up.reshape(w_key_up.shape[0], -1).T
    wvu = w_value_up.reshape(w_value_up.shape[0], -1).T
    wao = w_attn_out.reshape(-1, width)
    sg, su, dg, du = shared_gate.T, shared_up.T, dense_gate.T, dense_up.T
    rope = jnp.swapaxes(cache_rope_key, 1, 2)
    latent = wku.shape[1]
    ropew = wqr.shape[0]
    cap = max(2, -(-2 * rows * route_ids.shape[1] // n_ep))
    args = [
        lengths,
        tokens,
        cache_latent,
        rope,
        route_ids.T,
        route_weights.T,
        attn_gain.reshape(1, -1),
        wqn,
        wqr,
        wld,
        wkr,
        latent_gain.reshape(1, -1),
        wku,
        wvu,
        wao,
        ffn_gain.reshape(1, -1),
        expert_gate[0],
        expert_up[0],
        expert_down[0],
        sg,
        su,
        shared_down,
        dg,
        du,
        dense_down,
        branch_gate.astype(F32).reshape(1, -1),
    ]
    any_spec = pl.BlockSpec(memory_space=pl.ANY)
    vm = lambda a: pltpu.VMEM(a.shape, a.dtype)
    n1 = wqn.shape[0] + ropew + wld.shape[0]
    n2 = 2 * (sg.shape[0] + dg.shape[0])
    wide = latent + 128
    scratch = [
        vm(cache_latent),
        vm(rope),
        vm(args[4]),
        vm(args[5]),
        vm(args[6]),
        pltpu.VMEM((n1, width), BF16),
        vm(wkr),
        vm(args[11]),
        vm(wku),
        vm(wvu),
        vm(wao),
        vm(args[15]),
        vm(args[16]),
        vm(args[17]),
        vm(args[18]),
        pltpu.VMEM((n2, width), BF16),
        vm(shared_down),
        vm(dense_down),
        vm(args[25]),
        pltpu.VMEM((n_tp, rows, width), BF16),
        pltpu.VMEM((n_tp, rows, wide), BF16),
        pltpu.VMEM((n_tp, rows, wide), BF16),
        pltpu.VMEM((n_tp, rows, latent), BF16),
        pltpu.VMEM((n_tp, rows, latent), BF16),
        pltpu.VMEM((n_tp, rows, width), BF16),
        pltpu.VMEM((n_tp, rows, width), BF16),
        pltpu.VMEM((n_tp, rows, width), BF16),
        pltpu.VMEM((n_ep, cap, width), BF16),
        pltpu.VMEM((n_ep, cap, width), BF16),
        pltpu.VMEM((n_ep, cap, width), BF16),
        pltpu.VMEM((n_ep, cap, width), BF16),
        pltpu.VMEM((n_tp, rows, width), BF16),
        pltpu.VMEM((n_tp, rows, width), BF16),
        pltpu.VMEM((group, width), F32),
        pltpu.VMEM((n_ep * cap, width), F32),
        pltpu.VMEM((wide // 128, group, 128), F32),
        pltpu.VMEM((rows, 128), F32),
        pltpu.SemaphoreType.DMA((25,)),
        pltpu.SemaphoreType.DMA((8, max(n_tp, n_ep))),
        pltpu.SemaphoreType.DMA((8, max(n_tp, n_ep))),
    ]
    return pl.pallas_call(
        functools.partial(layer_kernel, n_tp, n_ep),
        out_shape=(
            jax.ShapeDtypeStruct((rows, width), BF16),
            jax.ShapeDtypeStruct((rows, latent), BF16),
            jax.ShapeDtypeStruct((rows, ropew), BF16),
        ),
        in_specs=[pl.BlockSpec(memory_space=pltpu.SMEM)] + [any_spec] * 25,
        out_specs=(pl.BlockSpec(memory_space=pltpu.VMEM),) * 3,
        scratch_shapes=scratch,
        compiler_params=pltpu.CompilerParams(
            collective_id=0, has_side_effects=True, vmem_limit_bytes=56 * 1024 * 1024
        ),
        name="layer",
    )(*args)


def solution(mesh):
    in_specs = (
        P(("ep", "tp"), None),
        P(("ep", "tp")),
        P(("ep", "tp"), None, None),
        P(("ep", "tp"), None, None),
        P("ep", None),
        P("ep", None),
        P(),
        P(None, "tp", None),
        P(None, "tp", None),
        P(None, "tp"),
        P(),
        P(),
        P(None, "tp", None),
        P(None, "tp", None),
        P("tp", None, None),
        P(),
        P(("ep", "tp"), None, None),
        P(("ep", "tp"), None, None),
        P(("ep", "tp"), None, None),
        P(None, "tp"),
        P(None, "tp"),
        P("tp", None),
        P(None, "tp"),
        P(None, "tp"),
        P("tp", None),
        P(),
    )
    out_specs = (P(("ep", "tp"), None), P(("ep", "tp"), None), P(("ep", "tp"), None))
    return jax.shard_map(local, mesh=mesh, in_specs=in_specs, out_specs=out_specs, check_vma=False)
```

time: 155 us -> 82.8 us (0.53)
  Pallas kernels: 0 us -> 76.8 us
  waiting for transfers between devices: 72.4 us -> 0 us
  starting transfers between devices: 43.1 us -> 0 us
  matrix products: 19 us -> 0 us
  local copies, waits for them, and re-layouts: 10.2 us -> 3.82 us
  other arithmetic: 7.66 us -> 1.29 us
    pallas_call x0 -> x1, Pallas kernels: none -> 76.8 us  [local(): pl.pallas_call(functools.partial(layer_kernel, n_tp, n_ep), out_shape=(ja...]
    all_to_all x9 -> x0, waiting for transfers between devices: 72.4 us -> none  [the longest x2 21.8 us: sent_and_summed(): tiles = lax.all_to_all(cut_along(shard, dim, peers), axis, 0, 0, tiled=True)]
    all_to_all x9 -> x0, starting transfers between devices: 43.1 us -> none  [the longest x2 13.4 us: copy_for_each(): lax.all_to_all(jnp.broadcast_to(shard[None], (peers, *shard.shape)), axis...]
    dot_general x19 -> x0, matrix products: 19 us -> none  [the longest x1 3.53 us: local(): jnp.einsum('bhr,blr->bhl', own_latent_q, cache_latent, preferred_element_...]
    reshape x6 -> x0, local copies, waits for them, and re-layouts: 4.1 us -> none  [the longest x2 2.55 us: cut_along(): return jnp.moveaxis(shard.reshape(*before, peers, -1, *after), dim, 0)]
    unnamed x38 -> x3, local copies, waits for them, and re-layouts: 1.11 us -> 3.82 us
    convert_element_type x8 -> x0, other arithmetic: 2.26 us -> none  [the longest x1 0.8 us: local(): normed = norm_rows(tokens, attn_gain).astype(jnp.bfloat16)]
    convert_element_type x5 -> x0, local copies, waits for them, and re-layouts: 2.26 us -> none  [the longest x1 0.78 us: local(): result = jnp.einsum('sxcf,xfd->sxcd', act_val, expert_down, preferred_ele...]
  transfers between devices with their start and end apart: 9 -> 0, of which waited for: 9 -> 0; matrix products, arithmetic and copies ran while one was open for 7% -> 0% of each run, Pallas kernels for 0% -> 0%
where the time goes in v1:
time: 82.8 us; the launch traced here: 82.5 us
  Pallas kernels  76.8 us (93%)
  local copies, waits for them, and re-layouts  3.82 us (5%)
  other arithmetic  1.29 us (2%)
    pallas_call x1, Pallas kernels, local(): pl.pallas_call(functools.partial(layer_kernel, n_tp, n_ep), out_shape=(ja...  76.8 us
    unnamed x3, local copies, waits for them, and re-layouts  3.82 us

profile of v1, /device:TPU:1, one launch (start us, length us, event | category | flops | bytes accessed | tf_op | source)
XLA Modules:
  0.0 82.5 jit_solution(17488948791376194964)
XLA Ops:
  0.6 1.3 %reshape.45 = f32[2048]{0:T(1024)} convert(bf16[2048]{0:T(1024)(128)(2,1)} %param.51) | non-fusion elementwise | flops 2048 | bytes 12288 | tf_op jit(solution)/shard_map/reshape | solution.py:480
  1.9 76.8 %layer.1 = (bf16[4,2048]{1,0:T(4,128)(2,1)}, bf16[4,512]{1,0:T(4,128)(2,1)}, bf16[4,32]{1,0:T(4,128)(2,1)}) custom-call(s32[4]{0:T(128)} %lengths.1, bf16[4,2048]{1,0:T(4,128)(2,1)} %tokens.1, bf16[4,1024,512]{2,1,0:T(8,128)(2,1)} %cache_h.1, bf16[4,32,1024]{2,1,0:T(8,128)(2,1)} %bitcast.32, s32[4,64]{1,0:T(4,128)} %bitcast.47, f32[4,64]{1,0:T(4,128)} %bitcast.48, ...), custom_call_target="tpu_custom_call" | custom-call | tf_op jit(solution)/shard_map/layer/pallas_call | solution.py:529
  78.7 1.3 %copy.32 = bf16[4,2048]{1,0:T(4,128)(2,1)} copy(bf16[4,2048]{1,0:T(4,128)(2,1)} %get-tuple-element.6) | data formatting | bytes 32768
  80.0 1.3 %copy.33 = bf16[4,512]{1,0:T(4,128)(2,1)} copy(bf16[4,512]{1,0:T(4,128)(2,1)} %get-tuple-element.7) | data formatting | bytes 8192
  81.3 1.2 %copy.34 = bf16[4,32]{1,0:T(4,128)(2,1)} copy(bf16[4,32]{1,0:T(4,128)(2,1)} %get-tuple-element.8) | data formatting | bytes 512

commit v2 on v1

--- a/solution.py
+++ b/solution.py
@@ -32,6 +32,12 @@
 
 def silu(v):
     return v / (1.0 + jnp.exp(-v))
+
+
+def finish_kernel(mixed, nlat, nrope, mixed_o, nlat_o, nrope_o):
+    mixed_o[...] = mixed[...]
+    nlat_o[...] = nlat[...]
+    nrope_o[...] = nrope[...]
 
 
 def layer_kernel(
@@ -91,6 +97,8 @@
     cs,
     cr,
     ds_,
+    dp,
+    dm,
     dr,
     ee,
     fs,
@@ -98,7 +106,10 @@
     gs,
     gr,
     hs,
+    hp,
+    hm,
     hr,
+    qbd,
     big,
     small,
     rf,
@@ -119,6 +130,9 @@
     scale = (nope + ropew) ** (-0.5)
 
     wide = latent + 128
+    n_z = n_tp // 2
+    core = lax.rem(me, 2)
+    place = lax.div(me, 2)
 
     def put(where, value):
         for k in range(value.shape[1] // 128):
@@ -128,7 +142,7 @@
         return jnp.concatenate([rf[k, where, :] for k in range(columns // 128)], axis=1)
 
     jobs = [
-        (tokens, xa.at[me]),
+        (tokens, xa.at[core, place]),
         (again_h, again),
         (wqn_h, w1.at[pl.ds(0, nope)]),
         (wqr_h, w1.at[pl.ds(nope, ropew)]),
@@ -175,48 +189,73 @@
     lax.fori_loop(1, n_tp, greet, 0)
     lax.fori_loop(1, n_ep, greet_ep, 0)
 
-    def hop(phase, i, axis, n, mine, src, dst):
-        to = lax.rem(mine + i, n)
+    def hop(phase, axis, to, src, dst):
         return pltpu.make_async_remote_copy(
-            src_ref=src(to),
-            dst_ref=dst.at[mine],
-            send_sem=send.at[phase, i],
-            recv_sem=recv.at[phase, i],
+            src_ref=src,
+            dst_ref=dst,
+            send_sem=send.at[phase],
+            recv_sem=recv.at[phase],
             device_id={axis: to},
             device_id_type=MESH,
         )
 
-    def start_all(phase, axis, n, mine, src, dst):
+    def wait_bytes(sem, like):
+        pltpu.make_async_copy(like, like, sem).wait()
+
+    def to_all(phase, axis, n, mine, src, dst):
         def body(i, _):
-            hop(phase, i, axis, n, mine, src, dst).start()
+            to = lax.rem(mine + n // 2 + i, n)
+
+            @pl.when(to != mine)
+            def _():
+                hop(phase, axis, to, src.at[to], dst.at[mine]).start()
+
             return 0
 
-        lax.fori_loop(1, n, body, 0)
-
-    def wait_all(phase, axis, n, mine, src, dst):
+        lax.fori_loop(0, n, body, 0)
+        dst[mine] = src[mine]
+
+    def await_all(phase, n, dst):
+        wait_bytes(recv.at[phase], dst.at[pl.ds(0, n - 1)])
+
+    def along_z(phase, pick, dst):
         def body(i, _):
-            hop(phase, i, axis, n, mine, src, dst).wait_recv()
+            up = lax.rem(place + i, n_z)
+            down = lax.rem(place + n_z - i, n_z)
+            hop(phase, "tp", 2 * up + core, pick(up), dst).start()
+
+            @pl.when(up != down)
+            def _():
+                hop(phase, "tp", 2 * down + core, pick(down), dst).start()
+
             return 0
 
-        lax.fori_loop(1, n, body, 0)
-
-    def wait_sent(phase, axis, n, mine, src, dst):
-        def body(i, _):
-            hop(phase, i, axis, n, mine, src, dst).wait_send()
-            return 0
-
-        lax.fori_loop(1, n, body, 0)
-
-    ex = [
-        (0, "tp", n_tp, me, lambda to: xa.at[me], xa),
-        (1, "tp", n_tp, me, lambda to: bs.at[to], br),
-        (2, "tp", n_tp, me, lambda to: cs.at[to], cr),
-        (3, "tp", n_tp, me, lambda to: ds_.at[to], dr),
-        (4, "tp", n_tp, me, lambda to: ee.at[me], ee),
-        (5, "ep", n_ep, grp, lambda to: fs.at[to], fr),
-        (6, "ep", n_ep, grp, lambda to: gs.at[to], gr),
-        (7, "tp", n_tp, me, lambda to: hs.at[to], hr),
-    ]
+        lax.fori_loop(0, n_z // 2, lambda j, x: body(n_z // 2 - j, x), 0)
+
+    def gather(phase, buf):
+        along_z(phase, lambda to: buf.at[core, place], buf.at[core, place])
+
+    def gather_rest(phase, buf):
+        wait_bytes(recv.at[phase], buf.at[0, pl.ds(0, n_z - 1)])
+        hop(phase + 1, "tp", 2 * place + 1 - core, buf.at[core], buf.at[core]).start()
+        wait_bytes(recv.at[phase + 1], buf.at[0])
+
+    def reduce_start(phase, src, pair):
+        hop(phase, "tp", 2 * place + 1 - core, src.at[1 - core], pair).start()
+
+    def reduce_rest(phase, src, pair, mid, dst):
+        wait_bytes(recv.at[phase], pair)
+        for z in range(n_z):
+            mid[z] = (src[core, z].astype(F32) + pair[z].astype(F32)).astype(BF16)
+        along_z(phase + 1, lambda to: mid.at[to], dst.at[place])
+        dst[place] = mid[place]
+
+    def reduce_sum(phase, dst):
+        wait_bytes(recv.at[phase + 1], dst.at[pl.ds(0, n_z - 1)])
+        total = dst[0].astype(F32)
+        for z in range(1, n_z):
+            total = total + dst[z].astype(F32)
+        return total
 
     lane = lax.broadcasted_iota(jnp.int32, (rows, 128), 1)
     rowi = lax.broadcasted_iota(jnp.int32, (rows, 128), 0)
@@ -240,31 +279,31 @@
 
     pl.semaphore_wait(barrier, (n_tp - 1) + (n_ep - 1))
     local[0].wait()
-    start_all(*ex[0])
+    gather(0, xa)
 
     local[1].wait()
     local[5].wait()
-    tok = xa[me].astype(F32)
+    tok = xa[core, place].astype(F32)
     own_normed = normed_rows(tok, again[...]).astype(BF16)
     krs[...] = jnp.zeros_like(krs)
+    qbd[...] = jnp.zeros_like(qbd)
     krs[:, 0:ropew] = nt(own_normed, wkr[...])
     new_rope = rotated(krs[...], cosv, sinv).astype(BF16).astype(F32)
     nrope_o[...] = new_rope[:, 0:ropew].astype(BF16)
     for i in (2, 3, 4, 6, 7):
         local[i].wait()
 
-    wait_all(*ex[0])
-    for t in range(n_tp):
-        big[pl.ds(rows * t, rows), :] = xa[t].astype(F32)
+    gather_rest(0, xa)
+    for t in range(n_tp):
+        big[pl.ds(rows * t, rows), :] = xa[t % 2, t // 2].astype(F32)
     normed = normed_rows(big[...], again[...]).astype(BF16)
     y = nt(normed, w1[...])
     ql = nn(y[:, 0:nope].astype(BF16), wku[...])
     put(pl.ds(0, group), jnp.concatenate([ql, y], axis=1))
     for t in range(n_tp):
         bs[t] = get(pl.ds(rows * t, rows), wide).astype(BF16)
-    start_all(*ex[1])
-    br[me] = bs[me]
-    wait_all(*ex[1])
+    to_all(2, "tp", n_tp, me, bs, br)
+    await_all(2, n_tp, br)
     for t in range(n_tp):
         put(pl.ds(rows * t, rows), br[t].astype(F32))
 
@@ -292,33 +331,46 @@
     local[8].wait()
     local[9].wait()
     n_heads = n_tp
-    outs = []
+    pairs = rows * n_heads
+    nlr = [new_latent[s : s + 1] for s in range(rows)]
+    qrots, owns = [], []
     for s in range(rows):
         q = get(pl.ds(s, n_heads, stride=rows), latent)
         qr = rf[latent // 128, pl.ds(s, n_heads, stride=rows), :]
-        qrot = rotated(qr, cosv[s : s + 1], sinv[s : s + 1]).astype(BF16)
-        sc = nt(q.astype(BF16), cache[s])
-        sc = (sc + nn(qrot[:, nope : nope + ropew], rope[s])) * scale
+        qbd[pl.ds(n_heads * s, n_heads), latent * s : latent * (s + 1)] = q.astype(BF16)
+        qrot = rotated(qr, cosv[s : s + 1], sinv[s : s + 1]).astype(BF16).astype(F32)
+        owns.append(
+            (
+                jnp.sum(q * nlr[s], axis=-1, keepdims=True)
+                + jnp.sum(qrot * nr_al[s : s + 1], axis=-1, keepdims=True)
+            )
+            * scale
+        )
+        shift = (ropew * s - nope) % 128
+        lnq = lax.broadcasted_iota(jnp.int32, qrot.shape, 1)
+        qrots.append(
+            jnp.where(lnq // ropew == s, pltpu.roll(qrot, shift, 1) if shift else qrot, 0.0)
+        )
+    qrbd = jnp.concatenate(qrots, axis=0).astype(BF16)
+    lhs = jnp.concatenate([cache[s] for s in range(rows)], axis=1)
+    sct = nt(lhs, qbd[...]).T
+    srope = nn(qrbd, rope[...])
+    for s in range(rows):
+        part = slice(n_heads * s, n_heads * (s + 1))
+        sc = (sct[part] + srope[part]) * scale
         col = lax.broadcasted_iota(jnp.int32, (n_heads, length), 1)
         sc = jnp.where(col < lengths[s], sc, -jnp.inf)
-        nls = new_latent[s : s + 1]
-        own = (
-            jnp.sum(q * nls, axis=-1, keepdims=True)
-            + jnp.sum(qrot.astype(F32) * nr_al[s : s + 1], axis=-1, keepdims=True)
-        ) * scale
+        own = owns[s]
         peak = jnp.maximum(jnp.max(sc, axis=-1, keepdims=True), own)
         pe = jnp.exp(sc - peak)
         oe = jnp.exp(own - peak)
         inv = 1.0 / (jnp.sum(pe, axis=-1, keepdims=True) + oe)
         pw = (pe * inv).astype(BF16)
         ow = (oe * inv).astype(BF16).astype(F32)
-        outs.append(nn(pw, cache[s]) + ow * nls)
-    for s in range(rows):
-        put(pl.ds(s, n_heads, stride=rows), outs[s])
-    for t in range(n_tp):
-        cs[t] = get(pl.ds(rows * t, rows), latent).astype(BF16)
-    start_all(*ex[2])
-    cr[me] = cs[me]
+        put(pl.ds(n_heads * s, n_heads), nn(pw, cache[s]) + ow * nlr[s])
+    for t in range(n_tp):
+        cs[t] = get(pl.ds(t, rows, stride=n_heads), latent).astype(BF16)
+    to_all(3, "tp", n_tp, me, cs, cr)
     for i in range(10, 16):
         local[i].wait()
 
@@ -343,41 +395,39 @@
     comb_hi = comb.astype(BF16)
     comb_lo = (comb - comb_hi.astype(F32)).astype(BF16)
 
-    wait_all(*ex[2])
+    await_all(3, n_tp, cr)
     for t in range(n_tp):
         put(pl.ds(rows * t, rows), cr[t].astype(F32))
     hv = nt(get(pl.ds(0, group), latent).astype(BF16), wvu[...]).astype(BF16)
     big[...] = nn(hv, wao[...])
     for t in range(n_tp):
-        ds_[t] = big[pl.ds(rows * t, rows), :].astype(BF16)
-    start_all(*ex[3])
-    dr[me] = ds_[me]
+        ds_[t % 2, t // 2] = big[pl.ds(rows * t, rows), :].astype(BF16)
+    reduce_start(4, ds_, dp)
     for i in range(16, len(jobs)):
         local[i].wait()
-    wait_all(*ex[3])
-    after = tok
-    total = jnp.zeros_like(tok)
-    for t in range(n_tp):
-        total = total + dr[t].astype(F32)
-    after = tok + total
-    ee[me] = normed_rows(after, fgain[...]).astype(BF16)
-    start_all(*ex[4])
-    wait_all(*ex[4])
-    for t in range(n_tp):
-        big[pl.ds(rows * t, rows), :] = ee[t].astype(F32)
+    reduce_rest(4, ds_, dp, dm, dr)
+    after = tok + reduce_sum(4, dr)
+    ee[core, place] = normed_rows(after, fgain[...]).astype(BF16)
+    gather(6, ee)
+    gather_rest(6, ee)
+    for t in range(n_tp):
+        big[pl.ds(rows * t, rows), :] = ee[t % 2, t // 2].astype(F32)
     ffn = big[...].astype(BF16)
     out = nn(disp, ffn)
-    mix = jax.nn.sigmoid(jnp.sum(big[...] * bg[...], axis=-1, keepdims=True))
+    gate = bg[...].astype(F32)
+    dots = big[:, 0:128] * gate[0:1]
+    for k in range(1, width // 128):
+        dots = dots + big[:, 128 * k : 128 * k + 128] * gate[k : k + 1]
+    mix = jax.nn.sigmoid(jnp.sum(dots, axis=-1, keepdims=True))
     small[...] = out
     for g in range(n_ep):
         fs[g] = small[pl.ds(cap * g, cap), :].astype(BF16)
-    start_all(*ex[5])
-    fr[grp] = fs[grp]
+    to_all(8, "ep", n_ep, grp, fs, fr)
     h = nt(ffn, w2[...])
     a, b = sg_h.shape[0], dg_h.shape[0]
     sact = (silu(h[:, 0:a]) * h[:, a : 2 * a]).astype(BF16)
     dact = (silu(h[:, 2 * a : 2 * a + b]) * h[:, 2 * a + b : 2 * a + 2 * b]).astype(BF16)
-    wait_all(*ex[5])
+    await_all(8, n_ep, fr)
     for g in range(n_ep):
         small[pl.ds(cap * g, cap), :] = fr[g].astype(F32)
     arrived = small[...].astype(BF16)
@@ -385,26 +435,28 @@
     small[...] = nn(act, ed[...])
     for g in range(n_ep):
         gs[g] = small[pl.ds(cap * g, cap), :].astype(BF16)
-    start_all(*ex[6])
-    gr[grp] = gs[grp]
+    to_all(9, "ep", n_ep, grp, gs, gr)
     big[...] = nn(sact, sd[...]) + mix * nn(dact, dd[...])
-    wait_all(*ex[6])
+    await_all(9, n_ep, gr)
     for g in range(n_ep):
         small[pl.ds(cap * g, cap), :] = gr[g].astype(F32)
     back = small[...].astype(BF16)
     big[...] += tn(comb_hi, back) + tn(comb_lo, back)
     for t in range(n_tp):
-        hs[t] = big[pl.ds(rows * t, rows), :].astype(BF16)
-    start_all(*ex[7])
-    hr[me] = hs[me]
-    for e in ex[:7]:
-        wait_sent(*e)
-    wait_all(*ex[7])
-    total = jnp.zeros_like(tok)
-    for t in range(n_tp):
-        total = total + hr[t].astype(F32)
+        hs[t % 2, t // 2] = big[pl.ds(rows * t, rows), :].astype(BF16)
+    reduce_start(10, hs, hp)
+    reduce_rest(10, hs, hp, hm, hr)
+    for phase, buf in ((0, xa), (6, ee)):
+        wait_bytes(send.at[phase], buf.at[0, pl.ds(0, n_z - 1)])
+        wait_bytes(send.at[phase + 1], buf.at[0])
+    for phase, n, buf in ((2, n_tp, bs), (3, n_tp, cs), (8, n_ep, fs), (9, n_ep, gs)):
+        wait_bytes(send.at[phase], buf.at[pl.ds(0, n - 1)])
+    for phase, buf in ((4, dp), (10, hp)):
+        wait_bytes(send.at[phase], buf)
+    wait_bytes(send.at[5], dm.at[pl.ds(0, n_z - 1)])
+    total = reduce_sum(10, hr)
     mixed_o[...] = (after + total).astype(BF16)
-    wait_sent(*ex[7])
+    wait_bytes(send.at[11], hm.at[pl.ds(0, n_z - 1)])
 
 
 def local(
@@ -447,7 +499,7 @@
     wvu = w_value_up.reshape(w_value_up.shape[0], -1).T
     wao = w_attn_out.reshape(-1, width)
     sg, su, dg, du = shared_gate.T, shared_up.T, dense_gate.T, dense_up.T
-    rope = jnp.swapaxes(cache_rope_key, 1, 2)
+    rope = jnp.swapaxes(cache_rope_key, 1, 2).reshape(-1, cache_rope_key.shape[1])
     latent = wku.shape[1]
     ropew = wqr.shape[0]
     cap = max(2, -(-2 * rows * route_ids.shape[1] // n_ep))
@@ -477,7 +529,7 @@
         dg,
         du,
         dense_down,
-        branch_gate.astype(F32).reshape(1, -1),
+        branch_gate.reshape(-1, 128),
     ]
     any_spec = pl.BlockSpec(memory_space=pl.ANY)
     vm = lambda a: pltpu.VMEM(a.shape, a.dtype)
@@ -504,29 +556,34 @@
         vm(shared_down),
         vm(dense_down),
         vm(args[25]),
-        pltpu.VMEM((n_tp, rows, width), BF16),
+        pltpu.VMEM((2, n_tp // 2, rows, width), BF16),
         pltpu.VMEM((n_tp, rows, wide), BF16),
         pltpu.VMEM((n_tp, rows, wide), BF16),
         pltpu.VMEM((n_tp, rows, latent), BF16),
         pltpu.VMEM((n_tp, rows, latent), BF16),
-        pltpu.VMEM((n_tp, rows, width), BF16),
-        pltpu.VMEM((n_tp, rows, width), BF16),
-        pltpu.VMEM((n_tp, rows, width), BF16),
+        pltpu.VMEM((2, n_tp // 2, rows, width), BF16),
+        pltpu.VMEM((n_tp // 2, rows, width), BF16),
+        pltpu.VMEM((n_tp // 2, rows, width), BF16),
+        pltpu.VMEM((n_tp // 2, rows, width), BF16),
+        pltpu.VMEM((2, n_tp // 2, rows, width), BF16),
         pltpu.VMEM((n_ep, cap, width), BF16),
         pltpu.VMEM((n_ep, cap, width), BF16),
         pltpu.VMEM((n_ep, cap, width), BF16),
         pltpu.VMEM((n_ep, cap, width), BF16),
-        pltpu.VMEM((n_tp, rows, width), BF16),
-        pltpu.VMEM((n_tp, rows, width), BF16),
+        pltpu.VMEM((2, n_tp // 2, rows, width), BF16),
+        pltpu.VMEM((n_tp // 2, rows, width), BF16),
+        pltpu.VMEM((n_tp // 2, rows, width), BF16),
+        pltpu.VMEM((n_tp // 2, rows, width), BF16),
+        pltpu.VMEM((-(-group // 128) * 128, rows * latent), BF16),
         pltpu.VMEM((group, width), F32),
         pltpu.VMEM((n_ep * cap, width), F32),
         pltpu.VMEM((wide // 128, group, 128), F32),
         pltpu.VMEM((rows, 128), F32),
         pltpu.SemaphoreType.DMA((25,)),
-        pltpu.SemaphoreType.DMA((8, max(n_tp, n_ep))),
-        pltpu.SemaphoreType.DMA((8, max(n_tp, n_ep))),
+        pltpu.SemaphoreType.DMA((12,)),
+        pltpu.SemaphoreType.DMA((12,)),
     ]
-    return pl.pallas_call(
+    found = pl.pallas_call(
         functools.partial(layer_kernel, n_tp, n_ep),
         out_shape=(
             jax.ShapeDtypeStruct((rows, width), BF16),
@@ -541,6 +598,14 @@
         ),
         name="layer",
     )(*args)
+    vmem = pl.BlockSpec(memory_space=pltpu.VMEM)
+    return pl.pallas_call(
+        finish_kernel,
+        out_shape=tuple(jax.ShapeDtypeStruct(a.shape, a.dtype) for a in found),
+        in_specs=[vmem] * 3,
+        out_specs=(vmem,) * 3,
+        name="finish",
+    )(*found)
 
 
 def solution(mesh):

time: 82.8 us -> 67.3 us (0.81)
  Pallas kernels: 76.8 us -> 66.5 us
  local copies, waits for them, and re-layouts: 3.82 us -> 0 us
  other arithmetic: 1.29 us -> 0 us
    pallas_call x1, Pallas kernels: 76.8 us -> 65.2 us  [local(): pl.pallas_call(functools.partial(layer_kernel, n_tp, n_ep), out_shape=(ja...]
    unnamed x3 -> x0, local copies, waits for them, and re-layouts: 3.82 us -> none
    pallas_call x0 -> x1, Pallas kernels: none -> 1.34 us  [local(): pl.pallas_call(finish_kernel, out_shape=tuple((jax.ShapeDtypeStruct(a.sha...]
    reshape x1 -> x0, other arithmetic: 1.29 us -> none  [local(): branch_gate.astype(F32).reshape(1, -1)]
where the time goes in v2:
time: 67.3 us; the launch traced here: 67.2 us
  Pallas kernels  66.5 us (99%)
    pallas_call x1, Pallas kernels, local(): pl.pallas_call(functools.partial(layer_kernel, n_tp, n_ep), out_shape=(ja...  65.2 us

profile of v2, /device:TPU:1, one launch (start us, length us, event | category | flops | bytes accessed | tf_op | source)
XLA Modules:
  0.0 67.2 jit_solution(13828468808803742298)
XLA Ops:
  0.6 65.2 %layer.1 = (bf16[4,2048]{1,0:T(4,128)(2,1)}, bf16[4,512]{1,0:T(4,128)(2,1)}, bf16[4,32]{1,0:T(4,128)(2,1)}) custom-call(s32[4]{0:T(128)} %lengths.1, bf16[4,2048]{1,0:T(4,128)(2,1)} %tokens.1, bf16[4,1024,512]{2,1,0:T(8,128)(2,1)} %cache_h.1, bf16[128,1024]{1,0:T(8,128)(2,1)} %bitcast.34, s32[4,64]{1,0:T(4,128)} %bitcast.49, f32[4,64]{1,0:T(4,128)} %bitcast.50, ...), custom_call_target="tpu_custom_call" | custom-call | tf_op jit(solution)/shard_map/layer/pallas_call | solution.py:586
  65.9 1.3 %finish.1 = (bf16[4,2048]{1,0:T(4,128)(2,1)}, bf16[4,512]{1,0:T(4,128)(2,1)}, bf16[4,32]{1,0:T(4,128)(2,1)}) custom-call(bf16[4,2048]{1,0:T(4,128)(2,1)} %get-tuple-element.6.mixed, bf16[4,512]{1,0:T(4,128)(2,1)} %get-tuple-element.7.nlat, bf16[4,32]{1,0:T(4,128)(2,1)} %get-tuple-element.8.nrope), custom_call_target="tpu_custom_call" | custom-call | tf_op jit(solution)/shard_map/finish/pallas_call | solution.py:602

commit v3 on v2

--- a/solution.py
+++ b/solution.py
@@ -43,7 +43,7 @@
 def layer_kernel(
     n_tp,
     n_ep,
-    lengths,
+    lengths_h,
     tokens,
     cache_h,
     rope_h,
@@ -72,6 +72,7 @@
     mixed_o,
     nlat_o,
     nrope_o,
+    lengths,
     cache,
     rope,
     ids,
@@ -109,7 +110,8 @@
     hp,
     hm,
     hr,
-    qbd,
+    sco,
+    prob,
     big,
     small,
     rf,
@@ -167,6 +169,7 @@
         (ed_h, ed),
         (sd_h, sd),
         (dd_h, dd),
+        (lengths_h, lengths),
     ]
     local = [pltpu.make_async_copy(s, d, lsem.at[i]) for i, (s, d) in enumerate(jobs)]
     for c in local:
@@ -202,35 +205,38 @@
     def wait_bytes(sem, like):
         pltpu.make_async_copy(like, like, sem).wait()
 
-    def to_all(phase, axis, n, mine, src, dst):
-        def body(i, _):
-            to = lax.rem(mine + n // 2 + i, n)
-
-            @pl.when(to != mine)
-            def _():
-                hop(phase, axis, to, src.at[to], dst.at[mine]).start()
-
-            return 0
-
-        lax.fori_loop(0, n, body, 0)
-        dst[mine] = src[mine]
+    def near(n):
+        return sorted(range(n), key=lambda d: (-min(d, n - d), d))
+
+    def to_all_tp(phase, src, dst):
+        for d in near(n_z):
+            for k in range(2):
+                if d or k:
+                    to = 2 * lax.rem(place + d, n_z) + lax.rem(core + k, 2)
+                    hop(phase, "tp", to, src.at[to], dst.at[me]).start()
+        dst[me] = src[me]
+
+    side = int(n_ep**0.5)
+    side = side if side * side == n_ep else 1
+    across = n_ep // side
+
+    def to_all_ep(phase, src, dst):
+        y, x = lax.div(grp, across), lax.rem(grp, across)
+        offsets = [(dy, dx) for dy in range(side) for dx in range(across) if dy or dx]
+        offsets.sort(key=lambda o: -min(o[0], side - o[0]) - min(o[1], across - o[1]))
+        for dy, dx in offsets:
+            to = lax.rem(y + dy, side) * across + lax.rem(x + dx, across)
+            hop(phase, "ep", to, src.at[to], dst.at[grp]).start()
+        dst[grp] = src[grp]
 
     def await_all(phase, n, dst):
         wait_bytes(recv.at[phase], dst.at[pl.ds(0, n - 1)])
 
     def along_z(phase, pick, dst):
-        def body(i, _):
-            up = lax.rem(place + i, n_z)
-            down = lax.rem(place + n_z - i, n_z)
-            hop(phase, "tp", 2 * up + core, pick(up), dst).start()
-
-            @pl.when(up != down)
-            def _():
-                hop(phase, "tp", 2 * down + core, pick(down), dst).start()
-
-            return 0
-
-        lax.fori_loop(0, n_z // 2, lambda j, x: body(n_z // 2 - j, x), 0)
+        for d in near(n_z):
+            if d:
+                z = lax.rem(place + d, n_z)
+                hop(phase, "tp", 2 * z + core, pick(z), dst).start()
 
     def gather(phase, buf):
         along_z(phase, lambda to: buf.at[core, place], buf.at[core, place])
@@ -257,6 +263,7 @@
             total = total + dst[z].astype(F32)
         return total
 
+    local[25].wait()
     lane = lax.broadcasted_iota(jnp.int32, (rows, 128), 1)
     rowi = lax.broadcasted_iota(jnp.int32, (rows, 128), 0)
     half = ropew // 2
@@ -286,7 +293,6 @@
     tok = xa[core, place].astype(F32)
     own_normed = normed_rows(tok, again[...]).astype(BF16)
     krs[...] = jnp.zeros_like(krs)
-    qbd[...] = jnp.zeros_like(qbd)
     krs[:, 0:ropew] = nt(own_normed, wkr[...])
     new_rope = rotated(krs[...], cosv, sinv).astype(BF16).astype(F32)
     nrope_o[...] = new_rope[:, 0:ropew].astype(BF16)
@@ -302,7 +308,7 @@
     put(pl.ds(0, group), jnp.concatenate([ql, y], axis=1))
     for t in range(n_tp):
         bs[t] = get(pl.ds(rows * t, rows), wide).astype(BF16)
-    to_all(2, "tp", n_tp, me, bs, br)
+    to_all_tp(2, bs, br)
     await_all(2, n_tp, br)
     for t in range(n_tp):
         put(pl.ds(rows * t, rows), br[t].astype(F32))
@@ -331,13 +337,12 @@
     local[8].wait()
     local[9].wait()
     n_heads = n_tp
-    pairs = rows * n_heads
     nlr = [new_latent[s : s + 1] for s in range(rows)]
     qrots, owns = [], []
     for s in range(rows):
         q = get(pl.ds(s, n_heads, stride=rows), latent)
         qr = rf[latent // 128, pl.ds(s, n_heads, stride=rows), :]
-        qbd[pl.ds(n_heads * s, n_heads), latent * s : latent * (s + 1)] = q.astype(BF16)
+        sco[s] = nt(q.astype(BF16), cache[s])
         qrot = rotated(qr, cosv[s : s + 1], sinv[s : s + 1]).astype(BF16).astype(F32)
         owns.append(
             (
@@ -352,12 +357,10 @@
             jnp.where(lnq // ropew == s, pltpu.roll(qrot, shift, 1) if shift else qrot, 0.0)
         )
     qrbd = jnp.concatenate(qrots, axis=0).astype(BF16)
-    lhs = jnp.concatenate([cache[s] for s in range(rows)], axis=1)
-    sct = nt(lhs, qbd[...]).T
     srope = nn(qrbd, rope[...])
+    own_w = []
     for s in range(rows):
-        part = slice(n_heads * s, n_heads * (s + 1))
-        sc = (sct[part] + srope[part]) * scale
+        sc = (sco[s] + srope[n_heads * s : n_heads * (s + 1)]) * scale
         col = lax.broadcasted_iota(jnp.int32, (n_heads, length), 1)
         sc = jnp.where(col < lengths[s], sc, -jnp.inf)
         own = owns[s]
@@ -365,12 +368,14 @@
         pe = jnp.exp(sc - peak)
         oe = jnp.exp(own - peak)
         inv = 1.0 / (jnp.sum(pe, axis=-1, keepdims=True) + oe)
-        pw = (pe * inv).astype(BF16)
-        ow = (oe * inv).astype(BF16).astype(F32)
-        put(pl.ds(n_heads * s, n_heads), nn(pw, cache[s]) + ow * nlr[s])
+        prob[s] = (pe * inv).astype(BF16)
+        own_w.append((oe * inv).astype(BF16).astype(F32))
+    for s in range(rows):
+        out = nn(prob[s], cache[s]) + own_w[s] * nlr[s]
+        put(pl.ds(n_heads * s, n_heads), out)
     for t in range(n_tp):
         cs[t] = get(pl.ds(t, rows, stride=n_heads), latent).astype(BF16)
-    to_all(3, "tp", n_tp, me, cs, cr)
+    to_all_tp(3, cs, cr)
     for i in range(10, 16):
         local[i].wait()
 
@@ -403,7 +408,7 @@
     for t in range(n_tp):
         ds_[t % 2, t // 2] = big[pl.ds(rows * t, rows), :].astype(BF16)
     reduce_start(4, ds_, dp)
-    for i in range(16, len(jobs)):
+    for i in range(16, 25):
         local[i].wait()
     reduce_rest(4, ds_, dp, dm, dr)
     after = tok + reduce_sum(4, dr)
@@ -422,7 +427,7 @@
     small[...] = out
     for g in range(n_ep):
         fs[g] = small[pl.ds(cap * g, cap), :].astype(BF16)
-    to_all(8, "ep", n_ep, grp, fs, fr)
+    to_all_ep(8, fs, fr)
     h = nt(ffn, w2[...])
     a, b = sg_h.shape[0], dg_h.shape[0]
     sact = (silu(h[:, 0:a]) * h[:, a : 2 * a]).astype(BF16)
@@ -435,7 +440,7 @@
     small[...] = nn(act, ed[...])
     for g in range(n_ep):
         gs[g] = small[pl.ds(cap * g, cap), :].astype(BF16)
-    to_all(9, "ep", n_ep, grp, gs, gr)
+    to_all_ep(9, gs, gr)
     big[...] = nn(sact, sd[...]) + mix * nn(dact, dd[...])
     await_all(9, n_ep, gr)
     for g in range(n_ep):
@@ -531,12 +536,13 @@
         dense_down,
         branch_gate.reshape(-1, 128),
     ]
-    any_spec = pl.BlockSpec(memory_space=pl.ANY)
+    hbm_spec = pl.BlockSpec(memory_space=pltpu.HBM)
     vm = lambda a: pltpu.VMEM(a.shape, a.dtype)
     n1 = wqn.shape[0] + ropew + wld.shape[0]
     n2 = 2 * (sg.shape[0] + dg.shape[0])
     wide = latent + 128
     scratch = [
+        pltpu.SMEM(lengths.shape, jnp.int32),
         vm(cache_latent),
         vm(rope),
         vm(args[4]),
@@ -574,12 +580,13 @@
         pltpu.VMEM((n_tp // 2, rows, width), BF16),
         pltpu.VMEM((n_tp // 2, rows, width), BF16),
         pltpu.VMEM((n_tp // 2, rows, width), BF16),
-        pltpu.VMEM((-(-group // 128) * 128, rows * latent), BF16),
+        pltpu.VMEM((rows, n_tp, cache_latent.shape[1]), F32),
+        pltpu.VMEM((rows, n_tp, cache_latent.shape[1]), BF16),
         pltpu.VMEM((group, width), F32),
         pltpu.VMEM((n_ep * cap, width), F32),
         pltpu.VMEM((wide // 128, group, 128), F32),
         pltpu.VMEM((rows, 128), F32),
-        pltpu.SemaphoreType.DMA((25,)),
+        pltpu.SemaphoreType.DMA((26,)),
         pltpu.SemaphoreType.DMA((12,)),
         pltpu.SemaphoreType.DMA((12,)),
     ]
@@ -590,20 +597,21 @@
             jax.ShapeDtypeStruct((rows, latent), BF16),
             jax.ShapeDtypeStruct((rows, ropew), BF16),
         ),
-        in_specs=[pl.BlockSpec(memory_space=pltpu.SMEM)] + [any_spec] * 25,
+        in_specs=[hbm_spec] * 26,
         out_specs=(pl.BlockSpec(memory_space=pltpu.VMEM),) * 3,
         scratch_shapes=scratch,
         compiler_params=pltpu.CompilerParams(
-            collective_id=0, has_side_effects=True, vmem_limit_bytes=56 * 1024 * 1024
+            collective_id=0, has_side_effects=True, vmem_limit_bytes=40 * 1024 * 1024
         ),
         name="layer",
-    )(*args)
+    )(*[pltpu.with_memory_space_constraint(a, pltpu.HBM) for a in args])
     vmem = pl.BlockSpec(memory_space=pltpu.VMEM)
     return pl.pallas_call(
         finish_kernel,
         out_shape=tuple(jax.ShapeDtypeStruct(a.shape, a.dtype) for a in found),
         in_specs=[vmem] * 3,
         out_specs=(vmem,) * 3,
+        compiler_params=pltpu.CompilerParams(vmem_limit_bytes=8 * 1024 * 1024),
         name="finish",
     )(*found)
 

time: 67.3 us -> 61.9 us (0.920)
  Pallas kernels: 66.5 us -> 61.2 us
    pallas_call x1, Pallas kernels: 65.2 us -> 60.6 us  [local(): pl.pallas_call(functools.partial(layer_kernel, n_tp, n_ep), out_shape=(ja...]
    pallas_call x1, Pallas kernels: 1.34 us -> 0.61 us  [local(): pl.pallas_call(finish_kernel, out_shape=tuple((jax.ShapeDtypeStruct(a.sha...]
where the time goes in v3:
time: 61.9 us; the launch traced here: 61.8 us
  Pallas kernels  61.2 us (99%)
  between operations  0.65 us (1%)
    pallas_call x1, Pallas kernels, local(): pl.pallas_call(functools.partial(layer_kernel, n_tp, n_ep), out_shape=(ja...  60.6 us

profile of v3, /device:TPU:1, one launch (start us, length us, event | category | flops | bytes accessed | tf_op | source)
XLA Modules:
  0.0 61.8 jit_solution(14332930476283415153)
XLA Ops:
  0.6 60.6 %layer.1 = (bf16[4,2048]{1,0:T(4,128)(2,1)S(1)}, bf16[4,512]{1,0:T(4,128)(2,1)S(1)}, bf16[4,32]{1,0:T(4,128)(2,1)S(1)}) custom-call(s32[4]{0:T(128)} %lengths_h.1, bf16[4,2048]{1,0:T(4,128)(2,1)} %tokens.1, bf16[4,1024,512]{2,1,0:T(8,128)(2,1)} %cache_h.1, bf16[128,1024]{1,0:T(8,128)(2,1)} %bitcast.34, s32[4,64]{1,0:T(4,128)} %bitcast.49, f32[4,64]{1,0:T(4,128)} %bitcast.50, ...), custom_call_target="tpu_custom_call" | custom-call | tf_op jit(solution)/shard_map/layer/pallas_call | solution.py:593
  61.2 0.6 finish.1

commit v4 on v3

--- a/solution.py
+++ b/solution.py
@@ -92,14 +92,13 @@
     sd,
     dd,
     bg,
+    xo,
     xa,
     bs,
     br,
     cs,
     cr,
     ds_,
-    dp,
-    dm,
     dr,
     ee,
     fs,
@@ -119,6 +118,7 @@
     lsem,
     send,
     recv,
+    each,
 ):
     me = lax.axis_index("tp")
     grp = lax.axis_index("ep")
@@ -135,6 +135,7 @@
     n_z = n_tp // 2
     core = lax.rem(me, 2)
     place = lax.div(me, 2)
+    other = 2 * place + 1 - core
 
     def put(where, value):
         for k in range(value.shape[1] // 128):
@@ -144,18 +145,18 @@
         return jnp.concatenate([rf[k, where, :] for k in range(columns // 128)], axis=1)
 
     jobs = [
-        (tokens, xa.at[core, place]),
+        (tokens, xo),
         (again_h, again),
-        (wqn_h, w1.at[pl.ds(0, nope)]),
-        (wqr_h, w1.at[pl.ds(nope, ropew)]),
-        (wld_h, w1.at[pl.ds(nope + ropew, latw)]),
+        (wqn_h, w1.at[core, pl.ds(0, nope)]),
+        (wqr_h, w1.at[core, pl.ds(nope, ropew)]),
+        (wld_h, w1.at[core, pl.ds(nope + ropew, latw)]),
         (wkr_h, wkr),
-        (wku_h, wku),
+        (wku_h, wku.at[core]),
         (lgain_h, lgain),
         (cache_h, cache),
         (rope_h, rope),
-        (wvu_h, wvu),
-        (wao_h, wao),
+        (wvu_h, wvu.at[core]),
+        (wao_h, wao.at[core]),
         (fgain_h, fgain),
         (ids_h, ids),
         (rw_h, rw),
@@ -172,32 +173,29 @@
         (lengths_h, lengths),
     ]
     local = [pltpu.make_async_copy(s, d, lsem.at[i]) for i, (s, d) in enumerate(jobs)]
+    barrier = pltpu.get_barrier_semaphore()
+
+    def near(n):
+        return sorted(range(n), key=lambda d: (-min(d, n - d), d))
+
+    for d in near(n_z):
+        for k in range(2):
+            if d or k:
+                to = 2 * lax.rem(place + d, n_z) + lax.rem(core + k, 2)
+                pl.semaphore_signal(barrier, inc=1, device_id={"tp": to}, device_id_type=MESH)
+    for d in near(n_ep):
+        if d:
+            to = lax.rem(grp + d, n_ep)
+            pl.semaphore_signal(barrier, inc=1, device_id={"ep": to}, device_id_type=MESH)
     for c in local:
         c.start()
 
-    barrier = pltpu.get_barrier_semaphore()
-
-    def greet(i, _):
-        pl.semaphore_signal(
-            barrier, inc=1, device_id={"tp": lax.rem(me + i, n_tp)}, device_id_type=MESH
-        )
-        return 0
-
-    def greet_ep(i, _):
-        pl.semaphore_signal(
-            barrier, inc=1, device_id={"ep": lax.rem(grp + i, n_ep)}, device_id_type=MESH
-        )
-        return 0
-
-    lax.fori_loop(1, n_tp, greet, 0)
-    lax.fori_loop(1, n_ep, greet_ep, 0)
-
-    def hop(phase, axis, to, src, dst):
+    def hop(phase, axis, to, src, dst, got=None):
         return pltpu.make_async_remote_copy(
             src_ref=src,
             dst_ref=dst,
             send_sem=send.at[phase],
-            recv_sem=recv.at[phase],
+            recv_sem=recv.at[phase] if got is None else got,
             device_id={axis: to},
             device_id_type=MESH,
         )
@@ -205,16 +203,13 @@
     def wait_bytes(sem, like):
         pltpu.make_async_copy(like, like, sem).wait()
 
-    def near(n):
-        return sorted(range(n), key=lambda d: (-min(d, n - d), d))
-
-    def to_all_tp(phase, src, dst):
+    def to_line(phase, src, dst):
         for d in near(n_z):
-            for k in range(2):
-                if d or k:
-                    to = 2 * lax.rem(place + d, n_z) + lax.rem(core + k, 2)
-                    hop(phase, "tp", to, src.at[to], dst.at[me]).start()
-        dst[me] = src[me]
+            z = lax.rem(place + d, n_z)
+            hop(phase, "tp", 2 * z + 1 - core, src.at[z], dst.at[place]).start()
+
+    def await_line(phase, dst):
+        wait_bytes(recv.at[phase], dst)
 
     side = int(n_ep**0.5)
     side = side if side * side == n_ep else 1
@@ -232,32 +227,43 @@
     def await_all(phase, n, dst):
         wait_bytes(recv.at[phase], dst.at[pl.ds(0, n - 1)])
 
-    def along_z(phase, pick, dst):
+
+    def gather(phase, row, buf):
+        own = buf.at[core, place]
         for d in near(n_z):
             if d:
                 z = lax.rem(place + d, n_z)
-                hop(phase, "tp", 2 * z + core, pick(z), dst).start()
-
-    def gather(phase, buf):
-        along_z(phase, lambda to: buf.at[core, place], buf.at[core, place])
-
-    def gather_rest(phase, buf):
-        wait_bytes(recv.at[phase], buf.at[0, pl.ds(0, n_z - 1)])
-        hop(phase + 1, "tp", 2 * place + 1 - core, buf.at[core], buf.at[core]).start()
+                hop(phase, "tp", 2 * z + core, own, own, each.at[row, d]).start()
+        hop(phase + 1, "tp", other, own, own).start()
+
+    def gather_rest(phase, row, buf):
+        for d in near(n_z):
+            if d:
+                block = buf.at[core, lax.rem(place + n_z - d, n_z)]
+                wait_bytes(each.at[row, d], block)
+                hop(phase + 1, "tp", other, block, block).start()
         wait_bytes(recv.at[phase + 1], buf.at[0])
 
-    def reduce_start(phase, src, pair):
-        hop(phase, "tp", 2 * place + 1 - core, src.at[1 - core], pair).start()
-
-    def reduce_rest(phase, src, pair, mid, dst):
-        wait_bytes(recv.at[phase], pair)
-        for z in range(n_z):
+    def reduce_start(phase, row, src, pair):
+        for d in near(n_z):
+            z = lax.rem(place + d, n_z)
+            hop(phase, "tp", other, src.at[1 - core, z], pair.at[z], each.at[row, d]).start()
+
+    def reduce_rest(phase, row, src, pair, mid, dst):
+        for d in near(n_z):
+            z = lax.rem(place + d, n_z)
+            wait_bytes(each.at[row, d], pair.at[z])
             mid[z] = (src[core, z].astype(F32) + pair[z].astype(F32)).astype(BF16)
-        along_z(phase + 1, lambda to: mid.at[to], dst.at[place])
-        dst[place] = mid[place]
+            if d:
+                hop(phase + 1, "tp", 2 * z + core, mid.at[z], dst.at[place]).start()
+            else:
+                dst[place] = mid[z]
 
     def reduce_sum(phase, dst):
         wait_bytes(recv.at[phase + 1], dst.at[pl.ds(0, n_z - 1)])
+        return line_sum(dst)
+
+    def line_sum(dst):
         total = dst[0].astype(F32)
         for z in range(1, n_z):
             total = total + dst[z].astype(F32)
@@ -286,32 +292,44 @@
 
     pl.semaphore_wait(barrier, (n_tp - 1) + (n_ep - 1))
     local[0].wait()
-    gather(0, xa)
+    for d in near(n_z):
+        to = 2 * lax.rem(place + d, n_z) + 1 - core
+        hop(0, "tp", to, xo, xa.at[place]).start()
+    shared = ((12, w1, (2, 3, 4)), (13, wku, (6,)), (14, wvu, (10,)), (15, wao, (11,)))
+    for phase, held, waits in shared:
+        for i in waits:
+            local[i].wait()
+        hop(phase, "tp", other, held.at[core], held.at[core]).start()
 
     local[1].wait()
     local[5].wait()
-    tok = xa[core, place].astype(F32)
+    tok = xo[...].astype(F32)
     own_normed = normed_rows(tok, again[...]).astype(BF16)
     krs[...] = jnp.zeros_like(krs)
     krs[:, 0:ropew] = nt(own_normed, wkr[...])
     new_rope = rotated(krs[...], cosv, sinv).astype(BF16).astype(F32)
     nrope_o[...] = new_rope[:, 0:ropew].astype(BF16)
-    for i in (2, 3, 4, 6, 7):
-        local[i].wait()
-
-    gather_rest(0, xa)
+    local[7].wait()
+
+    await_line(0, xa)
+    for phase, held, _ in shared[:2]:
+        wait_bytes(recv.at[phase], held.at[0])
+    half_rows = rows * n_z
+    part = big.at[pl.ds(0, half_rows)]
+    for z in range(n_z):
+        big[pl.ds(rows * z, rows), :] = xa[z].astype(F32)
+    normed = normed_rows(part[...], again[...]).astype(BF16)
+    y = nt(normed, w1[...].reshape(-1, width))
+    for k in range(2):
+        yk = y[:, 128 * k : 128 * k + 128]
+        ql = nn(yk[:, 0:nope].astype(BF16), wku[k])
+        put(pl.ds(0, half_rows), jnp.concatenate([ql, yk], axis=1))
+        for z in range(n_z):
+            bs[z, :, wide * k : wide * (k + 1)] = get(pl.ds(rows * z, rows), wide).astype(BF16)
+    to_line(2, bs, br)
+    await_line(2, br)
     for t in range(n_tp):
-        big[pl.ds(rows * t, rows), :] = xa[t % 2, t // 2].astype(F32)
-    normed = normed_rows(big[...], again[...]).astype(BF16)
-    y = nt(normed, w1[...])
-    ql = nn(y[:, 0:nope].astype(BF16), wku[...])
-    put(pl.ds(0, group), jnp.concatenate([ql, y], axis=1))
-    for t in range(n_tp):
-        bs[t] = get(pl.ds(rows * t, rows), wide).astype(BF16)
-    to_all_tp(2, bs, br)
-    await_all(2, n_tp, br)
-    for t in range(n_tp):
-        put(pl.ds(rows * t, rows), br[t].astype(F32))
+        put(pl.ds(rows * t, rows), br[t // 2, :, wide * (t % 2) : wide * (t % 2 + 1)].astype(F32))
 
     parts = []
     ln4 = lax.broadcasted_iota(jnp.int32, (rows, 128), 1)
@@ -319,7 +337,9 @@
     for k in range(latent // 128):
         acc = jnp.zeros((rows, 128), F32)
         for j in range(per):
-            piece = br[k * per + j][:, latent : latent + 128].astype(F32)
+            t = k * per + j
+            at = wide * (t % 2) + latent
+            piece = br[t // 2, :, at : at + 128].astype(F32)
             shift = (j * latw - (nope + ropew)) % 128
             if shift:
                 piece = pltpu.roll(piece, shift, 1)
@@ -374,9 +394,10 @@
         out = nn(prob[s], cache[s]) + own_w[s] * nlr[s]
         put(pl.ds(n_heads * s, n_heads), out)
     for t in range(n_tp):
-        cs[t] = get(pl.ds(t, rows, stride=n_heads), latent).astype(BF16)
-    to_all_tp(3, cs, cr)
-    for i in range(10, 16):
+        at = latent * (t % 2)
+        cs[t // 2, :, at : at + latent] = get(pl.ds(t, rows, stride=n_heads), latent).astype(BF16)
+    to_line(3, cs, cr)
+    for i in range(12, 16):
         local[i].wait()
 
     cap = fs.shape[1]
@@ -400,21 +421,27 @@
     comb_hi = comb.astype(BF16)
     comb_lo = (comb - comb_hi.astype(F32)).astype(BF16)
 
-    await_all(3, n_tp, cr)
-    for t in range(n_tp):
-        put(pl.ds(rows * t, rows), cr[t].astype(F32))
-    hv = nt(get(pl.ds(0, group), latent).astype(BF16), wvu[...]).astype(BF16)
-    big[...] = nn(hv, wao[...])
-    for t in range(n_tp):
-        ds_[t % 2, t // 2] = big[pl.ds(rows * t, rows), :].astype(BF16)
-    reduce_start(4, ds_, dp)
+    await_line(3, cr)
+    for phase, held, _ in shared[2:]:
+        wait_bytes(recv.at[phase], held.at[0])
+    total = None
+    for k in range(2):
+        for z in range(n_z):
+            put(pl.ds(rows * z, rows), cr[z, :, latent * k : latent * (k + 1)].astype(F32))
+        hv = nt(get(pl.ds(0, half_rows), latent).astype(BF16), wvu[k]).astype(BF16)
+        term = nn(hv, wao[k])
+        total = term if total is None else total + term
+    part[...] = total
+    for z in range(n_z):
+        ds_[z] = big[pl.ds(rows * z, rows), :].astype(BF16)
+    to_line(4, ds_, dr)
     for i in range(16, 25):
         local[i].wait()
-    reduce_rest(4, ds_, dp, dm, dr)
-    after = tok + reduce_sum(4, dr)
+    await_line(4, dr)
+    after = tok + line_sum(dr)
     ee[core, place] = normed_rows(after, fgain[...]).astype(BF16)
-    gather(6, ee)
-    gather_rest(6, ee)
+    gather(6, 0, ee)
+    gather_rest(6, 0, ee)
     for t in range(n_tp):
         big[pl.ds(rows * t, rows), :] = ee[t % 2, t // 2].astype(F32)
     ffn = big[...].astype(BF16)
@@ -449,16 +476,17 @@
     big[...] += tn(comb_hi, back) + tn(comb_lo, back)
     for t in range(n_tp):
         hs[t % 2, t // 2] = big[pl.ds(rows * t, rows), :].astype(BF16)
-    reduce_start(10, hs, hp)
-    reduce_rest(10, hs, hp, hm, hr)
-    for phase, buf in ((0, xa), (6, ee)):
-        wait_bytes(send.at[phase], buf.at[0, pl.ds(0, n_z - 1)])
-        wait_bytes(send.at[phase + 1], buf.at[0])
-    for phase, n, buf in ((2, n_tp, bs), (3, n_tp, cs), (8, n_ep, fs), (9, n_ep, gs)):
-        wait_bytes(send.at[phase], buf.at[pl.ds(0, n - 1)])
-    for phase, buf in ((4, dp), (10, hp)):
+    reduce_start(10, 1, hs, hp)
+    reduce_rest(10, 1, hs, hp, hm, hr)
+    wait_bytes(send.at[6], ee.at[0, pl.ds(0, n_z - 1)])
+    wait_bytes(send.at[7], ee.at[0])
+    for phase, buf in ((0, xa), (2, bs), (3, cs), (4, ds_)):
         wait_bytes(send.at[phase], buf)
-    wait_bytes(send.at[5], dm.at[pl.ds(0, n_z - 1)])
+    for phase, buf in ((8, fs), (9, gs)):
+        wait_bytes(send.at[phase], buf.at[pl.ds(0, n_ep - 1)])
+    wait_bytes(send.at[10], hp)
+    for phase, held, _ in shared:
+        wait_bytes(send.at[phase], held.at[0])
     total = reduce_sum(10, hr)
     mixed_o[...] = (after + total).astype(BF16)
     wait_bytes(send.at[11], hm.at[pl.ds(0, n_z - 1)])
@@ -548,12 +576,12 @@
         vm(args[4]),
         vm(args[5]),
         vm(args[6]),
-        pltpu.VMEM((n1, width), BF16),
+        pltpu.VMEM((2, n1, width), BF16),
         vm(wkr),
         vm(args[11]),
-        vm(wku),
-        vm(wvu),
-        vm(wao),
+        pltpu.VMEM((2, *wku.shape), BF16),
+        pltpu.VMEM((2, *wvu.shape), BF16),
+        pltpu.VMEM((2, *wao.shape), BF16),
         vm(args[15]),
         vm(args[16]),
         vm(args[17]),
@@ -562,13 +590,12 @@
         vm(shared_down),
         vm(dense_down),
         vm(args[25]),
-        pltpu.VMEM((2, n_tp // 2, rows, width), BF16),
-        pltpu.VMEM((n_tp, rows, wide), BF16),
-        pltpu.VMEM((n_tp, rows, wide), BF16),
-        pltpu.VMEM((n_tp, rows, latent), BF16),
-        pltpu.VMEM((n_tp, rows, latent), BF16),
-        pltpu.VMEM((2, n_tp // 2, rows, width), BF16),
+        pltpu.VMEM((rows, width), BF16),
         pltpu.VMEM((n_tp // 2, rows, width), BF16),
+        pltpu.VMEM((n_tp // 2, rows, 2 * wide), BF16),
+        pltpu.VMEM((n_tp // 2, rows, 2 * wide), BF16),
+        pltpu.VMEM((n_tp // 2, rows, 2 * latent), BF16),
+        pltpu.VMEM((n_tp // 2, rows, 2 * latent), BF16),
         pltpu.VMEM((n_tp // 2, rows, width), BF16),
         pltpu.VMEM((n_tp // 2, rows, width), BF16),
         pltpu.VMEM((2, n_tp // 2, rows, width), BF16),
@@ -587,8 +614,9 @@
         pltpu.VMEM((wide // 128, group, 128), F32),
         pltpu.VMEM((rows, 128), F32),
         pltpu.SemaphoreType.DMA((26,)),
-        pltpu.SemaphoreType.DMA((12,)),
-        pltpu.SemaphoreType.DMA((12,)),
+        pltpu.SemaphoreType.DMA((16,)),
+        pltpu.SemaphoreType.DMA((16,)),
+        pltpu.SemaphoreType.DMA((2, n_tp // 2)),
     ]
     found = pl.pallas_call(
         functools.partial(layer_kernel, n_tp, n_ep),

time: 61.9 us -> 59.3 us (0.958)
  Pallas kernels: 61.2 us -> 58.6 us
    pallas_call x1, Pallas kernels: 60.6 us -> 58 us  [local(): pl.pallas_call(functools.partial(layer_kernel, n_tp, n_ep), out_shape=(ja...]
where the time goes in v4:
time: 59.3 us; the launch traced here: 59.2 us
  Pallas kernels  58.6 us (99%)
  between operations  0.65 us (1%)
    pallas_call x1, Pallas kernels, local(): pl.pallas_call(functools.partial(layer_kernel, n_tp, n_ep), out_shape=(ja...  58 us

profile of v4, /device:TPU:1, one launch (start us, length us, event | category | flops | bytes accessed | tf_op | source)
XLA Modules:
  0.0 59.2 jit_solution(4169110481796369599)
XLA Ops:
  0.6 58.0 %layer.1 = (bf16[4,2048]{1,0:T(4,128)(2,1)S(1)}, bf16[4,512]{1,0:T(4,128)(2,1)S(1)}, bf16[4,32]{1,0:T(4,128)(2,1)S(1)}) custom-call(s32[4]{0:T(128)} %lengths_h.1, bf16[4,2048]{1,0:T(4,128)(2,1)} %tokens.1, bf16[4,1024,512]{2,1,0:T(8,128)(2,1)} %cache_h.1, bf16[128,1024]{1,0:T(8,128)(2,1)} %bitcast.34, s32[4,64]{1,0:T(4,128)} %bitcast.49, f32[4,64]{1,0:T(4,128)} %bitcast.50, ...), custom_call_target="tpu_custom_call" | custom-call | tf_op jit(solution)/shard_map/layer/pallas_call | solution.py:621
  58.6 0.6 %finish.1 = (bf16[4,2048]{1,0:T(4,128)(2,1)}, bf16[4,512]{1,0:T(4,128)(2,1)}, bf16[4,32]{1,0:T(4,128)(2,1)}) custom-call(bf16[4,2048]{1,0:T(4,128)(2,1)S(1)} %get-tuple-element.6.mixed, bf16[4,512]{1,0:T(4,128)(2,1)S(1)} %get-tuple-element.7.nlat, bf16[4,32]{1,0:T(4,128)(2,1)S(1)} %get-tuple-element.8.nrope), custom_call_target="tpu_custom_call" | custom-call | tf_op jit(solution)/shard_map/finish/pallas_call | solution.py:637

commit v5 on v4

--- a/solution.py
+++ b/solution.py
@@ -186,7 +186,7 @@
     for d in near(n_ep):
         if d:
             to = lax.rem(grp + d, n_ep)
-            pl.semaphore_signal(barrier, inc=1, device_id={"ep": to}, device_id_type=MESH)
+            pl.semaphore_signal(barrier, inc=1, device_id={"ep": to, "tp": other}, device_id_type=MESH)
     for c in local:
         c.start()
 
@@ -196,7 +196,7 @@
             dst_ref=dst,
             send_sem=send.at[phase],
             recv_sem=recv.at[phase] if got is None else got,
-            device_id={axis: to},
+            device_id={axis: to, "tp": other} if axis == "ep" else {axis: to},
             device_id_type=MESH,
         )
 
@@ -217,12 +217,11 @@
 
     def to_all_ep(phase, src, dst):
         y, x = lax.div(grp, across), lax.rem(grp, across)
-        offsets = [(dy, dx) for dy in range(side) for dx in range(across) if dy or dx]
+        offsets = [(dy, dx) for dy in range(side) for dx in range(across)]
         offsets.sort(key=lambda o: -min(o[0], side - o[0]) - min(o[1], across - o[1]))
         for dy, dx in offsets:
             to = lax.rem(y + dy, side) * across + lax.rem(x + dx, across)
             hop(phase, "ep", to, src.at[to], dst.at[grp]).start()
-        dst[grp] = src[grp]
 
     def await_all(phase, n, dst):
         wait_bytes(recv.at[phase], dst.at[pl.ds(0, n - 1)])
@@ -243,25 +242,6 @@
                 wait_bytes(each.at[row, d], block)
                 hop(phase + 1, "tp", other, block, block).start()
         wait_bytes(recv.at[phase + 1], buf.at[0])
-
-    def reduce_start(phase, row, src, pair):
-        for d in near(n_z):
-            z = lax.rem(place + d, n_z)
-            hop(phase, "tp", other, src.at[1 - core, z], pair.at[z], each.at[row, d]).start()
-
-    def reduce_rest(phase, row, src, pair, mid, dst):
-        for d in near(n_z):
-            z = lax.rem(place + d, n_z)
-            wait_bytes(each.at[row, d], pair.at[z])
-            mid[z] = (src[core, z].astype(F32) + pair[z].astype(F32)).astype(BF16)
-            if d:
-                hop(phase + 1, "tp", 2 * z + core, mid.at[z], dst.at[place]).start()
-            else:
-                dst[place] = mid[z]
-
-    def reduce_sum(phase, dst):
-        wait_bytes(recv.at[phase + 1], dst.at[pl.ds(0, n_z - 1)])
-        return line_sum(dst)
 
     def line_sum(dst):
         total = dst[0].astype(F32)
@@ -296,10 +276,14 @@
         to = 2 * lax.rem(place + d, n_z) + 1 - core
         hop(0, "tp", to, xo, xa.at[place]).start()
     shared = ((12, w1, (2, 3, 4)), (13, wku, (6,)), (14, wvu, (10,)), (15, wao, (11,)))
-    for phase, held, waits in shared:
-        for i in waits:
-            local[i].wait()
-        hop(phase, "tp", other, held.at[core], held.at[core]).start()
+
+    def share(parts):
+        for phase, held, waits in parts:
+            for i in waits:
+                local[i].wait()
+            hop(phase, "tp", other, held.at[core], held.at[core]).start()
+
+    share(shared[:2])
 
     local[1].wait()
     local[5].wait()
@@ -327,6 +311,9 @@
         for z in range(n_z):
             bs[z, :, wide * k : wide * (k + 1)] = get(pl.ds(rows * z, rows), wide).astype(BF16)
     to_line(2, bs, br)
+    share(shared[2:])
+    local[8].wait()
+    local[9].wait()
     await_line(2, br)
     for t in range(n_tp):
         put(pl.ds(rows * t, rows), br[t // 2, :, wide * (t % 2) : wide * (t % 2 + 1)].astype(F32))
@@ -354,8 +341,6 @@
         (lane_r >= nope) & (lane_r < nope + ropew), pltpu.roll(new_rope, nope, 1), 0.0
     )
 
-    local[8].wait()
-    local[9].wait()
     n_heads = n_tp
     nlr = [new_latent[s : s + 1] for s in range(rows)]
     qrots, owns = [], []
@@ -403,7 +388,7 @@
     cap = fs.shape[1]
     slots = n_ep * cap
     sl = lax.broadcasted_iota(jnp.int32, (slots, group), 0)
-    want = (sl // cap) * n_tp + me
+    want = (sl // cap) * n_tp + other
     hit = jnp.zeros((slots, group), F32)
     wgt = jnp.zeros((slots, group), F32)
     for k in range(ids_h.shape[0]):
@@ -446,20 +431,20 @@
         big[pl.ds(rows * t, rows), :] = ee[t % 2, t // 2].astype(F32)
     ffn = big[...].astype(BF16)
     out = nn(disp, ffn)
+    small[...] = out
+    for g in range(n_ep):
+        fs[g] = small[pl.ds(cap * g, cap), :].astype(BF16)
+    to_all_ep(8, fs, fr)
     gate = bg[...].astype(F32)
     dots = big[:, 0:128] * gate[0:1]
     for k in range(1, width // 128):
         dots = dots + big[:, 128 * k : 128 * k + 128] * gate[k : k + 1]
     mix = jax.nn.sigmoid(jnp.sum(dots, axis=-1, keepdims=True))
-    small[...] = out
-    for g in range(n_ep):
-        fs[g] = small[pl.ds(cap * g, cap), :].astype(BF16)
-    to_all_ep(8, fs, fr)
     h = nt(ffn, w2[...])
     a, b = sg_h.shape[0], dg_h.shape[0]
     sact = (silu(h[:, 0:a]) * h[:, a : 2 * a]).astype(BF16)
     dact = (silu(h[:, 2 * a : 2 * a + b]) * h[:, 2 * a + b : 2 * a + 2 * b]).astype(BF16)
-    await_all(8, n_ep, fr)
+    wait_bytes(recv.at[8], fr)
     for g in range(n_ep):
         small[pl.ds(cap * g, cap), :] = fr[g].astype(F32)
     arrived = small[...].astype(BF16)
@@ -469,25 +454,38 @@
         gs[g] = small[pl.ds(cap * g, cap), :].astype(BF16)
     to_all_ep(9, gs, gr)
     big[...] = nn(sact, sd[...]) + mix * nn(dact, dd[...])
-    await_all(9, n_ep, gr)
+    wait_bytes(recv.at[9], gr)
     for g in range(n_ep):
         small[pl.ds(cap * g, cap), :] = gr[g].astype(F32)
     back = small[...].astype(BF16)
     big[...] += tn(comb_hi, back) + tn(comb_lo, back)
-    for t in range(n_tp):
-        hs[t % 2, t // 2] = big[pl.ds(rows * t, rows), :].astype(BF16)
-    reduce_start(10, 1, hs, hp)
-    reduce_rest(10, 1, hs, hp, hm, hr)
+    def two(z):
+        both = big[pl.ds(pl.multiple_of(2 * rows * z, 2 * rows), 2 * rows), :]
+        low, high = both[0:rows], both[rows : 2 * rows]
+        return jnp.where(core == 0, low, high), jnp.where(core == 0, high, low)
+
+    order = [(d, lax.rem(place + d, n_z)) for d in near(n_z)]
+    for d, z in order:
+        hs[z] = two(z)[1].astype(BF16)
+        hop(10, "tp", other, hs.at[z], hp.at[z], each.at[1, d]).start()
+    for d, z in order:
+        wait_bytes(each.at[1, d], hp.at[z])
+        hm[z] = (two(z)[0] + hp[z].astype(F32)).astype(BF16)
+        if d:
+            hop(11, "tp", 2 * z + core, hm.at[z], hr.at[place]).start()
+        else:
+            hr[place] = hm[z]
     wait_bytes(send.at[6], ee.at[0, pl.ds(0, n_z - 1)])
     wait_bytes(send.at[7], ee.at[0])
     for phase, buf in ((0, xa), (2, bs), (3, cs), (4, ds_)):
         wait_bytes(send.at[phase], buf)
     for phase, buf in ((8, fs), (9, gs)):
-        wait_bytes(send.at[phase], buf.at[pl.ds(0, n_ep - 1)])
+        wait_bytes(send.at[phase], buf)
     wait_bytes(send.at[10], hp)
     for phase, held, _ in shared:
         wait_bytes(send.at[phase], held.at[0])
-    total = reduce_sum(10, hr)
+    wait_bytes(recv.at[11], hr.at[pl.ds(0, n_z - 1)])
+    total = line_sum(hr)
     mixed_o[...] = (after + total).astype(BF16)
     wait_bytes(send.at[11], hm.at[pl.ds(0, n_z - 1)])
 
@@ -603,7 +601,7 @@
         pltpu.VMEM((n_ep, cap, width), BF16),
         pltpu.VMEM((n_ep, cap, width), BF16),
         pltpu.VMEM((n_ep, cap, width), BF16),
-        pltpu.VMEM((2, n_tp // 2, rows, width), BF16),
+        pltpu.VMEM((n_tp // 2, rows, width), BF16),
         pltpu.VMEM((n_tp // 2, rows, width), BF16),
         pltpu.VMEM((n_tp // 2, rows, width), BF16),
         pltpu.VMEM((n_tp // 2, rows, width), BF16),

time: 59.3 us -> 58.6 us (0.988)
  Pallas kernels: 58.6 us -> 57.9 us
    pallas_call x1, Pallas kernels: 58 us -> 57.3 us  [local(): pl.pallas_call(functools.partial(layer_kernel, n_tp, n_ep), out_shape=(ja...]
where the time goes in v5:
time: 58.6 us
  Pallas kernels  57.9 us (99%)
  between operations  0.65 us (1%)
    pallas_call x1, Pallas kernels, local(): pl.pallas_call(functools.partial(layer_kernel, n_tp, n_ep), out_shape=(ja...  57.3 us

profile of v5, /device:TPU:1, one launch (start us, length us, event | category | flops | bytes accessed | tf_op | source)
XLA Modules:
  0.0 58.6 jit_solution(3535076052081676374)
XLA Ops:
  0.6 57.3 %layer.1 = (bf16[4,2048]{1,0:T(4,128)(2,1)S(1)}, bf16[4,512]{1,0:T(4,128)(2,1)S(1)}, bf16[4,32]{1,0:T(4,128)(2,1)S(1)}) custom-call(s32[4]{0:T(128)} %lengths_h.1, bf16[4,2048]{1,0:T(4,128)(2,1)} %tokens.1, bf16[4,1024,512]{2,1,0:T(8,128)(2,1)} %cache_h.1, bf16[128,1024]{1,0:T(8,128)(2,1)} %bitcast.34, s32[4,64]{1,0:T(4,128)} %bitcast.49, f32[4,64]{1,0:T(4,128)} %bitcast.50, ...), custom_call_target="tpu_custom_call" | custom-call | tf_op jit(solution)/shard_map/layer/pallas_call | solution.py:619
  57.9 0.6 %finish.1 = (bf16[4,2048]{1,0:T(4,128)(2,1)}, bf16[4,512]{1,0:T(4,128)(2,1)}, bf16[4,32]{1,0:T(4,128)(2,1)}) custom-call(bf16[4,2048]{1,0:T(4,128)(2,1)S(1)} %get-tuple-element.6.mixed, bf16[4,512]{1,0:T(4,128)(2,1)S(1)} %get-tuple-element.7.nlat, bf16[4,32]{1,0:T(4,128)(2,1)S(1)} %get-tuple-element.8.nrope), custom_call_target="tpu_custom_call" | custom-call | tf_op jit(solution)/shard_map/finish/pallas_call | solution.py:635

commit v6 on v5

--- a/solution.py
+++ b/solution.py
@@ -232,13 +232,13 @@
         for d in near(n_z):
             if d:
                 z = lax.rem(place + d, n_z)
-                hop(phase, "tp", 2 * z + core, own, own, each.at[row, d]).start()
+                hop(phase, "tp", 2 * z + 1 - core, own, own, each.at[row, d]).start()
         hop(phase + 1, "tp", other, own, own).start()
 
     def gather_rest(phase, row, buf):
         for d in near(n_z):
             if d:
-                block = buf.at[core, lax.rem(place + n_z - d, n_z)]
+                block = buf.at[1 - core, lax.rem(place + n_z - d, n_z)]
                 wait_bytes(each.at[row, d], block)
                 hop(phase + 1, "tp", other, block, block).start()
         wait_bytes(recv.at[phase + 1], buf.at[0])
@@ -275,7 +275,7 @@
     for d in near(n_z):
         to = 2 * lax.rem(place + d, n_z) + 1 - core
         hop(0, "tp", to, xo, xa.at[place]).start()
-    shared = ((12, w1, (2, 3, 4)), (13, wku, (6,)), (14, wvu, (10,)), (15, wao, (11,)))
+    shared = ((10, w1, (2, 3, 4)), (11, wku, (6,)), (12, wvu, (10,)), (13, wao, (11,)))
 
     def share(parts):
         for phase, held, waits in parts:
@@ -310,11 +310,11 @@
         put(pl.ds(0, half_rows), jnp.concatenate([ql, yk], axis=1))
         for z in range(n_z):
             bs[z, :, wide * k : wide * (k + 1)] = get(pl.ds(rows * z, rows), wide).astype(BF16)
-    to_line(2, bs, br)
+    to_line(1, bs, br)
     share(shared[2:])
     local[8].wait()
     local[9].wait()
-    await_line(2, br)
+    await_line(1, br)
     for t in range(n_tp):
         put(pl.ds(rows * t, rows), br[t // 2, :, wide * (t % 2) : wide * (t % 2 + 1)].astype(F32))
 
@@ -381,7 +381,7 @@
     for t in range(n_tp):
         at = latent * (t % 2)
         cs[t // 2, :, at : at + latent] = get(pl.ds(t, rows, stride=n_heads), latent).astype(BF16)
-    to_line(3, cs, cr)
+    to_line(2, cs, cr)
     for i in range(12, 16):
         local[i].wait()
 
@@ -406,7 +406,7 @@
     comb_hi = comb.astype(BF16)
     comb_lo = (comb - comb_hi.astype(F32)).astype(BF16)
 
-    await_line(3, cr)
+    await_line(2, cr)
     for phase, held, _ in shared[2:]:
         wait_bytes(recv.at[phase], held.at[0])
     total = None
@@ -419,14 +419,14 @@
     part[...] = total
     for z in range(n_z):
         ds_[z] = big[pl.ds(rows * z, rows), :].astype(BF16)
-    to_line(4, ds_, dr)
+    to_line(3, ds_, dr)
     for i in range(16, 25):
         local[i].wait()
-    await_line(4, dr)
+    await_line(3, dr)
     after = tok + line_sum(dr)
     ee[core, place] = normed_rows(after, fgain[...]).astype(BF16)
-    gather(6, 0, ee)
-    gather_rest(6, 0, ee)
+    gather(4, 0, ee)
+    gather_rest(4, 0, ee)
     for t in range(n_tp):
         big[pl.ds(rows * t, rows), :] = ee[t % 2, t // 2].astype(F32)
     ffn = big[...].astype(BF16)
@@ -434,7 +434,7 @@
     small[...] = out
     for g in range(n_ep):
         fs[g] = small[pl.ds(cap * g, cap), :].astype(BF16)
-    to_all_ep(8, fs, fr)
+    to_all_ep(6, fs, fr)
     gate = bg[...].astype(F32)
     dots = big[:, 0:128] * gate[0:1]
     for k in range(1, width // 128):
@@ -444,7 +444,7 @@
     a, b = sg_h.shape[0], dg_h.shape[0]
     sact = (silu(h[:, 0:a]) * h[:, a : 2 * a]).astype(BF16)
     dact = (silu(h[:, 2 * a : 2 * a + b]) * h[:, 2 * a + b : 2 * a + 2 * b]).astype(BF16)
-    wait_bytes(recv.at[8], fr)
+    wait_bytes(recv.at[6], fr)
     for g in range(n_ep):
         small[pl.ds(cap * g, cap), :] = fr[g].astype(F32)
     arrived = small[...].astype(BF16)
@@ -452,9 +452,9 @@
     small[...] = nn(act, ed[...])
     for g in range(n_ep):
         gs[g] = small[pl.ds(cap * g, cap), :].astype(BF16)
-    to_all_ep(9, gs, gr)
+    to_all_ep(7, gs, gr)
     big[...] = nn(sact, sd[...]) + mix * nn(dact, dd[...])
-    wait_bytes(recv.at[9], gr)
+    wait_bytes(recv.at[7], gr)
     for g in range(n_ep):
         small[pl.ds(cap * g, cap), :] = gr[g].astype(F32)
     back = small[...].astype(BF16)
@@ -467,27 +467,27 @@
     order = [(d, lax.rem(place + d, n_z)) for d in near(n_z)]
     for d, z in order:
         hs[z] = two(z)[1].astype(BF16)
-        hop(10, "tp", other, hs.at[z], hp.at[z], each.at[1, d]).start()
+        hop(8, "tp", other, hs.at[z], hp.at[z], each.at[1, d]).start()
     for d, z in order:
         wait_bytes(each.at[1, d], hp.at[z])
         hm[z] = (two(z)[0] + hp[z].astype(F32)).astype(BF16)
         if d:
-            hop(11, "tp", 2 * z + core, hm.at[z], hr.at[place]).start()
+            hop(9, "tp", 2 * z + core, hm.at[z], hr.at[place]).start()
         else:
             hr[place] = hm[z]
-    wait_bytes(send.at[6], ee.at[0, pl.ds(0, n_z - 1)])
-    wait_bytes(send.at[7], ee.at[0])
-    for phase, buf in ((0, xa), (2, bs), (3, cs), (4, ds_)):
+    wait_bytes(send.at[4], ee.at[0, pl.ds(0, n_z - 1)])
+    wait_bytes(send.at[5], ee.at[0])
+    for phase, buf in ((0, xa), (1, bs), (2, cs), (3, ds_)):
         wait_bytes(send.at[phase], buf)
-    for phase, buf in ((8, fs), (9, gs)):
+    for phase, buf in ((6, fs), (7, gs)):
         wait_bytes(send.at[phase], buf)
-    wait_bytes(send.at[10], hp)
+    wait_bytes(send.at[8], hp)
     for phase, held, _ in shared:
         wait_bytes(send.at[phase], held.at[0])
-    wait_bytes(recv.at[11], hr.at[pl.ds(0, n_z - 1)])
+    wait_bytes(recv.at[9], hr.at[pl.ds(0, n_z - 1)])
     total = line_sum(hr)
     mixed_o[...] = (after + total).astype(BF16)
-    wait_bytes(send.at[11], hm.at[pl.ds(0, n_z - 1)])
+    wait_bytes(send.at[9], hm.at[pl.ds(0, n_z - 1)])
 
 
 def local(
@@ -612,8 +612,8 @@
         pltpu.VMEM((wide // 128, group, 128), F32),
         pltpu.VMEM((rows, 128), F32),
         pltpu.SemaphoreType.DMA((26,)),
-        pltpu.SemaphoreType.DMA((16,)),
-        pltpu.SemaphoreType.DMA((16,)),
+        pltpu.SemaphoreType.DMA((14,)),
+        pltpu.SemaphoreType.DMA((14,)),
         pltpu.SemaphoreType.DMA((2, n_tp // 2)),
     ]
     found = pl.pallas_call(

time: 58.6 us -> 58.3 us (level)
  no operation moved by 1% of the time
where the time goes in v6:
time: 58.3 us; the launch traced here: 58.2 us
  Pallas kernels  57.6 us (99%)
  between operations  0.65 us (1%)
    pallas_call x1, Pallas kernels, local(): pl.pallas_call(functools.partial(layer_kernel, n_tp, n_ep), out_shape=(ja...  56.9 us

profile of v6, /device:TPU:1, one launch (start us, length us, event | category | flops | bytes accessed | tf_op | source)
XLA Modules:
  0.0 58.2 jit_solution(4808644864784510423)
XLA Ops:
  0.6 56.9 %layer.1 = (bf16[4,2048]{1,0:T(4,128)(2,1)S(1)}, bf16[4,512]{1,0:T(4,128)(2,1)S(1)}, bf16[4,32]{1,0:T(4,128)(2,1)S(1)}) custom-call(s32[4]{0:T(128)} %lengths_h.1, bf16[4,2048]{1,0:T(4,128)(2,1)} %tokens.1, bf16[4,1024,512]{2,1,0:T(8,128)(2,1)} %cache_h.1, bf16[128,1024]{1,0:T(8,128)(2,1)} %bitcast.34, s32[4,64]{1,0:T(4,128)} %bitcast.49, f32[4,64]{1,0:T(4,128)} %bitcast.50, ...), custom_call_target="tpu_custom_call" | custom-call | tf_op jit(solution)/shard_map/layer/pallas_call | solution.py:619
  57.6 0.6 %finish.1 = (bf16[4,2048]{1,0:T(4,128)(2,1)}, bf16[4,512]{1,0:T(4,128)(2,1)}, bf16[4,32]{1,0:T(4,128)(2,1)}) custom-call(bf16[4,2048]{1,0:T(4,128)(2,1)S(1)} %get-tuple-element.6.mixed, bf16[4,512]{1,0:T(4,128)(2,1)S(1)} %get-tuple-element.7.nlat, bf16[4,32]{1,0:T(4,128)(2,1)S(1)} %get-tuple-element.8.nrope), custom_call_target="tpu_custom_call" | custom-call | tf_op jit(solution)/shard_map/finish/pallas_call | solution.py:635
